TPU v7x, 256 devices: a whole 4x4x8 slice. The times are simulated.
256 devices in a mesh: ep: 32 (over z, x), tp: 8 (over y, core).
Axes of the slice: x: 4, y: 4, z: 8, core: 2. Of those that a mesh axis runs over, the one named last changes fastest.
Arguments:
- tokens: bfloat16 [2048, 4096], P('ep'), may hold values from -6 to 6
- state_in: float32 [2048, 4096], P('ep', 'tp'), may hold values from -6 to 6
- conv_in: bfloat16 [2048, 3, 4096], P('ep', None, 'tp'), may hold values from -6 to 6
- mix_gain: bfloat16 [4096], replicated, may hold values from 0.099609375 to 1.8984375
- rnn_weight: bfloat16 [4096, 4096], P('ep', 'tp'), may hold values from -0.09375 to 0.09375
- gate_weight: bfloat16 [4096, 4096], P('ep', 'tp'), may hold values from -0.09375 to 0.09375
- conv_weight: bfloat16 [4, 4096], P(None, 'tp'), may hold values from -3 to 3
- rate_weight: bfloat16 [16, 256, 256], P('tp'), may hold values from -0.375 to 0.375
- input_weight: bfloat16 [16, 256, 256], P('tp'), may hold values from -0.375 to 0.375
- rate_param: float32 [4096], P('tp'), may hold values from 1 to 6
- out_weight: bfloat16 [4096, 4096], P('tp'), may hold values from -0.09375 to 0.09375
- moe_gain: bfloat16 [4096], replicated, may hold values from 0.099609375 to 1.8984375
- expert_gate: bfloat16 [32, 4096, 2048], P('ep', None, 'tp'), may hold values from -0.09375 to 0.09375
- expert_up: bfloat16 [32, 4096, 2048], P('ep', None, 'tp'), may hold values from -0.09375 to 0.09375
- expert_down: bfloat16 [32, 2048, 4096], P('ep', 'tp'), may hold values from -0.125 to 0.125
- routes: int32 [2048, 2], P('ep'), may hold values from 0 to 31, all different within a row; in each aligned block of 64 rows (0 to 63, 64 to 127, ...) at most 8 rows name the same one
- route_prob: float32 [2048, 2], P('ep'), may hold values from 0.1 to 1
Outputs:
- layer_out: bfloat16 [2048, 4096], P('ep', 'tp')
- state_out: float32 [2048, 4096], P('ep', 'tp')
- conv_out: bfloat16 [2048, 3, 4096], P('ep', None, 'tp')
Inputs may be any that keep to these rules, and one draw needn't show every extreme that they name: `routes`: the 2 experts of a sequence differ. Among the rows of one index of ep no expert is named more than 8 times, and in every draw some expert is named exactly 8 times there.
All inputs are finite; a program needn't handle non-finite values.
Results may differ from a plain program's by a relative error of at most 0.014.
Values may be sent and summed in bfloat16 or wider, within the bound.
A program may use at most 64 MiB of HBM per device.

v0:
```python
import jax
import jax.numpy as jnp
from jax import lax
from jax.sharding import PartitionSpec as P


def side_by_side(arrays, axis, dim, along):
    ends, at = ([], 0)
    for a in arrays[:-1]:
        at += a.shape[along]
        ends.append(at)
    both = jnp.concatenate(arrays, axis=along)
    return tuple(jnp.split(lax.all_gather(both, axis, axis=dim, tiled=True), ends, axis=along))


def over_pieces(shard, axis):
    parts = lax.all_gather(shard, axis).astype(jnp.float32)
    return parts.sum(axis=0)


def in_blocks(shard, dim, size):
    before, after = (shard.shape[:dim], shard.shape[dim + 1 :])
    return jnp.moveaxis(shard.reshape(*before, size, -1, *after), dim, 0)


def sum_at_owner(shard, axis, dim):
    size = lax.axis_size(axis)
    parts = lax.all_to_all(in_blocks(shard, dim, size), axis, 0, 0, tiled=True)
    return jnp.sum(parts.astype(jnp.float32), axis=0)


def rms_scale(values, gain):
    scale = lax.rsqrt(jnp.mean(values * values, axis=-1, keepdims=True) + 1e-06)
    return values * scale * gain.astype(jnp.float32)


def slot_targets(route_ids, experts, capacity):
    flat_ids = route_ids.reshape(-1)
    onehot = (flat_ids[:, None] == jnp.arange(experts, dtype=jnp.int32)[None, :]).astype(jnp.int32)
    before = jnp.cumsum(onehot, axis=0) - onehot
    slot_ids = jnp.sum(before * onehot, axis=1)
    return flat_ids * capacity + slot_ids


def block_map(conv, weight):
    rows = conv.shape[0]
    blocks = weight.shape[0]
    parts = conv.reshape(rows, blocks, weight.shape[1])
    mapped = jnp.einsum("snc,ncd->snd", parts, weight, preferred_element_type=jnp.float32)
    return mapped.reshape(rows, blocks * weight.shape[2])


def shards(
    tokens,
    state_in,
    conv_in,
    mix_gain,
    rnn_weight,
    gate_weight,
    conv_weight,
    rate_weight,
    input_weight,
    rate_param,
    out_weight,
    moe_gain,
    expert_gate,
    expert_up,
    expert_down,
    routes,
    route_prob,
):
    group_rows = tokens.shape[0]
    model_width = tokens.shape[1]
    base = tokens.astype(jnp.float32)
    normed = rms_scale(base, mix_gain).astype(jnp.bfloat16)
    pieces = side_by_side((rnn_weight, gate_weight), "ep", 0, 1)
    proj_x = jnp.dot(normed, pieces[0], preferred_element_type=jnp.float32)
    proj_y = jnp.dot(normed, pieces[1], preferred_element_type=jnp.float32)
    moved = proj_x.astype(jnp.bfloat16)
    conv_out = jnp.concatenate([conv_in[:, 1:], moved[:, None, :]], axis=1)
    taps = conv_weight.astype(jnp.float32)
    history = conv_in.astype(jnp.float32)
    mixed_in = (
        history[:, 0] * taps[0]
        + history[:, 1] * taps[1]
        + history[:, 2] * taps[2]
        + moved.astype(jnp.float32) * taps[3]
    )
    conv = mixed_in.astype(jnp.bfloat16)
    rate = jax.nn.sigmoid(block_map(conv, rate_weight))
    in_gate = jax.nn.sigmoid(block_map(conv, input_weight))
    log_decay = -8.0 * rate * jax.nn.softplus(-rate_param)
    state_out = jnp.exp(log_decay) * state_in + jnp.sqrt(
        -jnp.expm1(2.0 * log_decay)
    ) * in_gate * conv.astype(jnp.float32)
    gated = (state_out * jax.nn.gelu(proj_y, approximate=True)).astype(jnp.bfloat16)
    partial_out = jnp.dot(gated, out_weight, preferred_element_type=jnp.float32)
    mixed = base + over_pieces(partial_out.astype(jnp.bfloat16), "tp").astype(jnp.float32)
    normed2 = rms_scale(mixed, moe_gain).astype(jnp.bfloat16)
    experts = lax.axis_size("ep")
    topk = routes.shape[1]
    capacity = max(2, 2 * group_rows * topk // experts)
    targets = slot_targets(routes, experts, capacity)
    dispatch = (
        jnp.arange(experts * capacity, dtype=jnp.int32)[:, None] == targets[None, :]
    ).astype(jnp.bfloat16)
    repeated = jnp.repeat(normed2, topk, axis=0)
    send = jnp.dot(dispatch, repeated, preferred_element_type=jnp.float32).astype(jnp.bfloat16)
    send = send.reshape(experts, capacity, model_width)
    received = lax.all_to_all(send, "ep", split_axis=0, concat_axis=0, tiled=True)
    flat_rows = received.reshape(-1, model_width)
    gate_part = jnp.dot(flat_rows, expert_gate[0], preferred_element_type=jnp.float32)
    up_part = jnp.dot(flat_rows, expert_up[0], preferred_element_type=jnp.float32)
    hidden = (jax.nn.silu(gate_part) * up_part).astype(jnp.bfloat16)
    result = jnp.dot(hidden, expert_down[0], preferred_element_type=jnp.float32)
    partial_experts = result.reshape(received.shape[0], received.shape[1], model_width)
    reduced = sum_at_owner(partial_experts.astype(jnp.bfloat16), "tp", 2).astype(jnp.bfloat16)
    returned = lax.all_to_all(reduced, "ep", split_axis=0, concat_axis=0, tiled=True)
    share = returned.shape[2]
    picked = jnp.einsum(
        "rj,rd->jd",
        dispatch,
        returned.reshape(experts * capacity, share),
        preferred_element_type=jnp.float32,
    )
    weights = route_prob / jnp.sum(route_prob, axis=1, keepdims=True)
    experts_sum = jnp.sum(picked.reshape(group_rows, topk, share) * weights[:, :, None], axis=1)
    own_columns = lax.dynamic_slice_in_dim(mixed, lax.axis_index("tp") * share, share, 1)
    layer_out = (own_columns + experts_sum).astype(jnp.bfloat16)
    return (layer_out, state_out, conv_out)


def solution(mesh):
    in_specs = (
        P("ep", None),
        P("ep", "tp"),
        P("ep", None, "tp"),
        P(),
        P("ep", "tp"),
        P("ep", "tp"),
        P(None, "tp"),
        P("tp", None, None),
        P("tp", None, None),
        P("tp"),
        P("tp", None),
        P(),
        P("ep", None, "tp"),
        P("ep", None, "tp"),
        P("ep", "tp", None),
        P("ep", None),
        P("ep", None),
    )
    out_specs = (P("ep", "tp"), P("ep", "tp"), P("ep", None, "tp"))
    return jax.shard_map(shards, mesh=mesh, in_specs=in_specs, out_specs=out_specs, check_vma=False)
```

profile of v0, /device:TPU:1, one launch (start us, length us, event | category | flops | bytes accessed | tf_op | source)
XLA Modules:
  0.0 295.5 jit_solution(8402819260702172702)
XLA Ops:
  7.2 1.9 pad_maximum_fusion
  9.2 0.7 convert_element_type.63
  9.9 1.0 convert_element_type.61
  10.8 1.2 fusion.43
  12.1 0.7 fusion.98
  12.8 0.8 fusion.104
  13.6 97.8 %all-gather.4.cloned.1.call-done = bf16[4096,1024]{1,0:T(8,128)(2,1)} async-done(((bf16[128,1024]{1,0:T(8,128)(2,1)}), bf16[4096,1024]{1,0:T(8,128)(2,1)}) %all-gather.4.cloned.1.call-update) | async-done | bytes 8388624 | tf_op jit(solution)/shard_map/all_gather | solution.py:13
  111.5 3.9 %fusion.82 = (bf16[64,512]{1,0:T(8,128)(2,1)S(1)}, bf16[64,512]{1,0:T(8,128)(2,1)}) fusion(f32[64,3,512]{2,0,1:T(8,128)S(1)} %convert_element_type.61, f32[512]{0:T(512)S(1)} %bitcast.106, f32[512]{0:T(512)S(1)} %bitcast.105, f32[512]{0:T(512)S(1)} %bitcast.104, f32[512]{0:T(512)S(1)} %bitcast.103, bf16[4096,1024]{1,0:T(8,128)(2,1)} %all-gather.4.cloned.1.call-done, ...), kind=kOutput, calls=%fused_computation.63 | convolution fusion | flops 269811712 | bytes 5267712 | tf_op jit(solution)/shard_map/dot_general | solution.py:77
  115.7 0.2 fusion.35
  115.9 0.4 copy-done.6
  116.5 6.1 %convolution_convert_fusion.2 = bf16[64,4096]{1,0:T(8,128)(2,1)} fusion(bf16[512,4096]{1,0:T(8,128)(2,1)} %param.27, f32[64,512]{1,0:T(8,128)S(1)} %multiply_add_fusion, bf16[4096,1024]{1,0:T(8,128)(2,1)} %all-gather.4.cloned.1.call-done, bf16[64,4096]{1,0:T(8,128)(2,1)S(1)} %copy-done.2, f32[4096]{0:T(1024)S(1)} %convert_element_type.63, ...), kind=kOutput, calls=%fused_computation.4 | convolution fusion | flops 538509312 | bytes 9584896 | tf_op jit(solution)/shard_map/dot_general | solution.py:97
  123.4 32.3 %all-gather.6.cloned.1.call-done = bf16[512,4096]{1,0:T(8,128)(2,1)} async-done(((bf16[64,4096]{1,0:T(8,128)(2,1)}), bf16[512,4096]{1,0:T(8,128)(2,1)}) %all-gather.6.cloned.1.call-update) | async-done | bytes 4194320 | tf_op jit(solution)/shard_map/all_gather | solution.py:17
  155.7 3.0 %convert_reduce_fusion = f32[64,4096]{1,0:T(8,128)S(1)} fusion(bf16[8,64,4096]{2,1,0:T(8,128)(2,1)} %bitcast.97), kind=kLoop, calls=%fused_computation | loop fusion | flops 3932160 | bytes 5242880 | tf_op jit(solution)/shard_map/reduce_sum | solution.py:18
  158.7 0.2 multiply_reduce_fusion
  159.2 2.0 broadcast_in_dim.4
  161.2 2.3 reshape.102
  163.4 1.9 fusion
  165.3 58.8 %all_to_all.15 = bf16[32,8,4096]{2,1,0:T(8,128)(2,1)S(1)} all-to-all(bf16[32,8,4096]{2,1,0:T(8,128)(2,1)S(1)} %fusion), channel_id=1, replica_groups=mesh['ep'=32,'tp'=8] {'ep'}, dimensions={0} | all-to-all | bytes 4194304 | tf_op jit(solution)/shard_map/all_to_all | solution.py:110
  224.1 1.3 copy-done.1
  225.5 0.7 fusion.8
  226.2 5.9 %convolution_convert_fusion.1 = bf16[32,8,4096]{2,1,0:T(8,128)(2,1)} fusion(bf16[1,256,4096]{2,1,0:T(8,128)(2,1)S(1)} %copy-done, bf16[1,4096,256]{2,1,0:T(8,128)(2,1)} %param.30, bf16[32,8,4096]{2,1,0:T(8,128)(2,1)} %copy-done.1, f32[256,256]{1,0:T(8,128)S(1)} %fusion.8), kind=kOutput, calls=%fused_computation.2 | convolution fusion | flops 1075183616 | bytes 8650752 | tf_op jit(solution)/shard_map/dot_general | solution.py:115
  232.1 3.1 %copy.52 = bf16[32,8,8,512]{3,1,0,2:T(8,128)(2,1)} copy(bf16[32,8,8,512]{3,1,2,0:T(8,128)(2,1)} %bitcast.96) | data formatting | bytes 4194304 | tf_op jit(solution)/shard_map/reshape | solution.py:23
  235.2 6.3 %all-to-all-start.1 = ((bf16[8,32,8,512]{3,2,1,0:T(8,128)(2,1)}), bf16[8,32,8,512]{3,2,1,0:T(8,128)(2,1)}, u32[]{:S(2)}, u32[]{:S(2)}) async-start(bf16[8,32,8,512]{3,2,1,0:T(8,128)(2,1)} %bitcast.95), calls=%async_computation.1 | async-start | bytes 4194304 | tf_op jit(solution)/shard_map/all_to_all | solution.py:28
  241.6 26.3 %all-to-all-done.1 = bf16[8,32,8,512]{3,2,1,0:T(8,128)(2,1)} async-done(((bf16[8,32,8,512]{3,2,1,0:T(8,128)(2,1)}), bf16[8,32,8,512]{3,2,1,0:T(8,128)(2,1)}, u32[]{:S(2)}, u32[]{:S(2)}) %all-to-all-start.1) | async-done | bytes 2097184 | tf_op jit(solution)/shard_map/all_to_all | solution.py:28
  267.9 2.7 reduce_sum.70
  270.6 5.3 %all-to-all-start.2 = ((bf16[32,8,512]{2,1,0:T(8,128)(2,1)}), bf16[32,8,512]{2,1,0:T(8,128)(2,1)S(1)}, u32[]{:S(2)}, u32[]{:S(2)}) async-start(bf16[32,8,512]{2,1,0:T(8,128)(2,1)} %reduce_sum.70), calls=%async_computation.2 | async-start | bytes 524288 | tf_op jit(solution)/shard_map/all_to_all | solution.py:118
  275.9 0.7 iota_compare_fusion.1
  276.6 1.4 eq.47
  278.0 1.5 pad_maximum_fusion.1
  279.6 7.4 %all-to-all-done.2 = bf16[32,8,512]{2,1,0:T(8,128)(2,1)S(1)} async-done(((bf16[32,8,512]{2,1,0:T(8,128)(2,1)}), bf16[32,8,512]{2,1,0:T(8,128)(2,1)S(1)}, u32[]{:S(2)}, u32[]{:S(2)}) %all-to-all-start.2) | async-done | bytes 262176 | tf_op jit(solution)/shard_map/all_to_all | solution.py:118
  287.0 1.0 fusion.22
  288.0 0.7 add_convert_fusion
  (44 shorter events, 1.5 us)
Async XLA Ops:
  7.2 219.0 %copy-start = (bf16[1,256,4096]{2,1,0:T(8,128)(2,1)S(1)}, bf16[1,256,4096]{2,1,0:T(8,128)(2,1)}, u32[]{:S(2)}) copy-start(bf16[1,256,4096]{2,1,0:T(8,128)(2,1)} %param.31) | copy-start | bytes 6291460
  7.2 104.3 %all-gather.4.cloned.1.call-start = ((), (), s32[]{:S(2)}) async-start(), calls=%async_computation.3 | async-start | bytes 8650752 | tf_op jit(solution)/shard_map/all_gather | solution.py:13
  9.1 146.6 %all-gather.6.cloned.1.call-start = ((), (), s32[]{:S(2)}) async-start(), calls=%async_computation.4 | async-start | bytes 4718592 | tf_op jit(solution)/shard_map/all_gather | solution.py:17
  111.5 3.9 %copy-start.10 = (bf16[2,256,256]{2,1,0:T(8,128)(2,1)S(1)}, bf16[2,256,256]{2,1,0:T(8,128)(2,1)}, u32[]{:S(2)}) copy-start(bf16[2,256,256]{2,1,0:T(8,128)(2,1)} %param.24) | copy-start | bytes 786436
  111.5 4.2 %copy-start.11 = (bf16[2,256,256]{2,1,0:T(8,128)(2,1)S(1)}, bf16[2,256,256]{2,1,0:T(8,128)(2,1)}, u32[]{:S(2)}) copy-start(bf16[2,256,256]{2,1,0:T(8,128)(2,1)} %param.25) | copy-start | bytes 786436
  115.4 0.9 copy-start.6
  115.4 1.1 copy-start.2
  116.5 6.1 %copy-start.5 = (f32[64,512]{1,0:T(8,128)}, f32[64,512]{1,0:T(8,128)S(1)}, u32[]{:S(2)}) copy-start(f32[64,512]{1,0:T(8,128)S(1)} %multiply_add_fusion) | copy-start | bytes 393220
  116.5 6.1 %copy-start.7 = (bf16[4096]{0:T(1024)(128)(2,1)S(1)}, bf16[4096]{0:T(1024)(128)(2,1)}, u32[]{:S(2)}) copy-start(bf16[4096]{0:T(1024)(128)(2,1)} %param.28) | copy-start | bytes 24580
  116.5 6.1 %copy-start.9 = (s32[64,2]{0,1:T(2,128)S(1)}, s32[64,2]{0,1:T(2,128)}, u32[]{:S(2)}) copy-start(s32[64,2]{0,1:T(2,128)} %param.32) | copy-start | bytes 1540
  155.7 3.0 %copy-start.3 = (bf16[64,4096]{1,0:T(8,128)(2,1)S(1)}, bf16[64,4096]{1,0:T(8,128)(2,1)}, u32[]{:S(2)}) copy-start(bf16[64,4096]{1,0:T(8,128)(2,1)} %param.17) | copy-start | bytes 1572868
  165.3 60.1 %copy-start.4 = (bf16[1,4096,256]{2,1,0:T(8,128)(2,1)S(1)}, bf16[1,4096,256]{2,1,0:T(8,128)(2,1)}, u32[]{:S(2)}) copy-start(bf16[1,4096,256]{2,1,0:T(8,128)(2,1)} %param.29) | copy-start | bytes 6291460
  224.1 1.3 copy-start.1
  235.2 32.7 %all-to-all-start.1 = ((bf16[8,32,8,512]{3,2,1,0:T(8,128)(2,1)}), bf16[8,32,8,512]{3,2,1,0:T(8,128)(2,1)}, u32[]{:S(2)}, u32[]{:S(2)}) async-start(bf16[8,32,8,512]{3,2,1,0:T(8,128)(2,1)} %bitcast.95), calls=%async_computation.1 | async-start | bytes 4194304 | tf_op jit(solution)/shard_map/all_to_all | solution.py:28
  241.5 36.5 %copy-start.8 = (f32[64,2]{0,1:T(2,128)S(1)}, f32[64,2]{0,1:T(2,128)}, u32[]{:S(2)}) copy-start(f32[64,2]{0,1:T(2,128)} %param.33) | copy-start | bytes 1540
  241.5 36.5 %slice-start = ((bf16[64,3,512]{2,0,1:T(8,128)(2,1)}), bf16[64,2,512]{2,0,1:T(8,128)(2,1)S(1)}, s32[]{:S(2)}) async-start(bf16[64,3,512]{2,0,1:T(8,128)(2,1)} %param.19), calls=%async_computation.5 | async-start | bytes 262144 | tf_op jit(solution)/shard_map/slice | solution.py:80
  270.6 16.4 %all-to-all-start.2 = ((bf16[32,8,512]{2,1,0:T(8,128)(2,1)}), bf16[32,8,512]{2,1,0:T(8,128)(2,1)S(1)}, u32[]{:S(2)}, u32[]{:S(2)}) async-start(bf16[32,8,512]{2,1,0:T(8,128)(2,1)} %reduce_sum.70), calls=%async_computation.2 | async-start | bytes 524288 | tf_op jit(solution)/shard_map/all_to_all | solution.py:118
Sparse Core Ops, SparseCore 0:
  10.6 100.8 all-gather.3
  122.8 32.8 all-gather.5
where the time goes:
time: 297 us; the launch traced here: 295 us
  waiting for transfers between devices  164 us (55%)
  blocking collectives  58.8 us (20%)
  matrix products  20 us (7%)
  other arithmetic  15.1 us (5%)
  between operations  14.3 us (5%)
  local copies, waits for them, and re-layouts  11.8 us (4%)
  starting transfers between devices  11.7 us (4%)
    all_gather x1, waiting for transfers between devices, side_by_side(): lax.all_gather(both, axis, axis=dim, tiled=True)  97.8 us
    all_to_all x1, blocking collectives, shards(): lax.all_to_all(send, 'ep', split_axis=0, concat_axis=0, tiled=True)  58.8 us
    all_gather x1, waiting for transfers between devices, over_pieces(): parts = lax.all_gather(shard, axis).astype(jnp.float32)  32.3 us
    all_to_all x1, waiting for transfers between devices, sum_at_owner(): parts = lax.all_to_all(in_blocks(shard, dim, size), axis, 0, 0, tiled=True)  26.3 us
    all_to_all x1, waiting for transfers between devices, shards(): lax.all_to_all(reduced, 'ep', split_axis=0, concat_axis=0, tiled=True)  7.38 us
    all_to_all x1, starting transfers between devices, sum_at_owner(): parts = lax.all_to_all(in_blocks(shard, dim, size), axis, 0, 0, tiled=True)  6.35 us
    dot_general x1, matrix products, shards(): partial_out = jnp.dot(gated, out_weight, preferred_element_type=jnp.float32)  6.08 us
  transfers between devices with their start and end apart: 4, of which 4 were waited for; matrix products, arithmetic and copies ran while one was open for 3% of the time, Pallas kernels for 0%

commit v1 on v0

v1 whole, which is shorter than its diff:
```python
import functools

import jax
import jax.numpy as jnp
from jax import lax
from jax.experimental import pallas as pl
from jax.experimental.pallas import tpu as pltpu
from jax.sharding import PartitionSpec as P

NX = 4
NY = 4
NC = 2
MESH = pl.DeviceIdType.MESH
F32 = jnp.float32
BF16 = jnp.bfloat16


def dot(a, b):
    return jnp.dot(a, b, preferred_element_type=F32)


def dot_t(a, b):
    return lax.dot_general(a, b, (((0,), (0,)), ((), ())), preferred_element_type=F32)


def layer_kernel(
    tokens,
    hist,
    state_in,
    mix_gain,
    rnn_w,
    gate_w,
    tap,
    rate_w,
    input_w,
    rate_param,
    moe_gain,
    routes,
    prob,
    out_w_hbm,
    eg_hbm,
    eu_hbm,
    ed_hbm,
    layer_out,
    state_out,
    moved_out,
    out_w,
    wgu,
    wd,
    nrm,
    acts,
    wbuf,
    pbuf,
    rs_send,
    rs_recv,
    os_send,
    os_recv,
    oy_send,
    oy_recv,
    sd,
    gbuf,
    xg,
    acc,
    d_send,
    d_recv,
    qf,
    q_send,
    fw_recv,
    fin_recv,
    back_send,
    back_recv,
    local_sem,
    w_ssem,
    w_rsem,
    a_ssem,
    a_rsem,
    ad_ssem,
    ad_rsem,
    rs_ssem,
    rs_rsem,
    os_ssem,
    os_rsem,
    oy_ssem,
    oy_rsem,
    s_ssem,
    s_rsem,
    ag_ssem,
    ag_rsem,
    d_ssem,
    d_rsem,
    q_ssem,
    fw_rsem,
    fin_rsem,
    b_ssem,
    b_rsem,
):
    rows, width = tokens.shape
    chan = rnn_w.shape[1]
    ks = rnn_w.shape[0]
    ep_n = width // ks
    nz = ep_n // NX
    half_z = nz // 2
    tp_n = NY * NC
    kz = width // nz
    kh = kz // 2
    ff = wd.shape[0]
    cap = sd.shape[0] // ep_n // 2
    ch = chan // 2
    slots = ep_n * cap

    ep = lax.axis_index("ep")
    tp = lax.axis_index("tp")
    z = ep // NX
    x = ep % NX
    y = tp // NC
    c = tp % NC
    other = (c + 1) % NC

    def epid(zz, xx):
        return (zz % nz) * NX + xx % NX

    def tpid(yy, cc):
        return (yy % NY) * NC + cc

    partner = tpid(y, other)
    started = []

    def send(src, dst, ssem, rsem, to_ep, to_tp):
        copy = pltpu.make_async_remote_copy(
            src_ref=src,
            dst_ref=dst,
            send_sem=ssem,
            recv_sem=rsem,
            device_id=(to_ep, to_tp),
            device_id_type=MESH,
        )
        copy.start()
        started.append(copy)

    def arrived(dst, ssem, rsem):
        pltpu.make_async_remote_copy(
            src_ref=dst,
            dst_ref=dst,
            send_sem=ssem,
            recv_sem=rsem,
            device_id=(ep, partner),
            device_id_type=MESH,
        ).wait_recv()

    load_ow = pltpu.make_async_copy(out_w_hbm, out_w, local_sem.at[0])
    load_eg = pltpu.make_async_copy(eg_hbm.at[0], wgu.at[:, pl.ds(0, ff)], local_sem.at[1])
    load_eu = pltpu.make_async_copy(eu_hbm.at[0], wgu.at[:, pl.ds(ff, ff)], local_sem.at[2])
    load_ed = pltpu.make_async_copy(ed_hbm.at[0], wd, local_sem.at[3])
    load_ow.start()
    load_eg.start()
    load_eu.start()
    load_ed.start()

    barrier = pltpu.get_barrier_semaphore()

    @pl.loop(1, ep_n)
    def _(i):
        pl.semaphore_signal(
            barrier, inc=1, device_id=((ep + i) % ep_n, tp), device_id_type=MESH
        )

    @pl.loop(1, tp_n)
    def _(i):
        pl.semaphore_signal(
            barrier, inc=1, device_id=(ep, (tp + i) % tp_n), device_id_type=MESH
        )

    base = tokens[...].astype(F32)
    scale = lax.rsqrt(jnp.mean(base * base, axis=-1, keepdims=True) + 1e-06)
    normed = (base * scale * mix_gain[...].astype(F32)).astype(BF16)
    for k in range(2 * nz):
        nrm[k] = normed[:, k * kh : (k + 1) * kh]
    wbuf[0, pl.ds(x * ks, ks), :] = rnn_w[...]
    wbuf[1, pl.ds(x * ks, ks), :] = gate_w[...]
    for h in range(2):
        acts[h, pl.ds(z * rows, rows), :] = nrm[2 * z + h]

    pl.semaphore_wait(barrier, ep_n - 1 + tp_n - 1)

    own_w = (rnn_w, gate_w)

    def w_slot(part, xx):
        return wbuf.at[part, pl.ds((xx % NX) * ks, ks), :]

    for n, (part, d) in enumerate(((0, 1), (1, -1), (1, 1), (0, -1))):
        send(
            own_w[part],
            w_slot(part, x),
            w_ssem.at[n],
            w_rsem.at[part, x],
            epid(z, x + d + NX),
            tp,
        )

    order = []
    for i in range(half_z, 0, -1):
        order.append(i)
        if i < half_z:
            order.append(nz - i)
    for i in order:
        to_z = (z + i) % nz
        send(
            nrm.at[2 * to_z + c],
            acts.at[c, pl.ds(z * rows, rows), :],
            a_ssem.at[i],
            a_rsem.at[z],
            epid(to_z, x),
            tp,
        )
    for i in reversed(order):
        from_z = (z + nz - i) % nz
        block = acts.at[c, pl.ds(from_z * rows, rows), :]
        arrived(block, a_ssem.at[i], a_rsem.at[from_z])
        send(block, block, ad_ssem.at[i], ad_rsem.at[from_z], ep, partner)

    left = (x + NX - 1) % NX
    right = (x + 1) % NX
    far = (x + 2) % NX
    arrived(w_slot(0, left), w_ssem.at[0], w_rsem.at[0, left])
    send(w_slot(0, left), w_slot(0, left), w_ssem.at[4], w_rsem.at[0, left], epid(z, right), tp)
    arrived(w_slot(1, right), w_ssem.at[0], w_rsem.at[1, right])
    send(w_slot(1, right), w_slot(1, right), w_ssem.at[5], w_rsem.at[1, right], epid(z, left), tp)
    arrived(w_slot(1, left), w_ssem.at[0], w_rsem.at[1, left])
    arrived(w_slot(0, right), w_ssem.at[0], w_rsem.at[0, right])
    for i in reversed(order):
        from_z = (z + nz - i) % nz
        block = acts.at[other, pl.ds(from_z * rows, rows), :]
        arrived(block, ad_ssem.at[i], ad_rsem.at[from_z])
    arrived(w_slot(0, far), w_ssem.at[0], w_rsem.at[0, far])
    arrived(w_slot(1, far), w_ssem.at[0], w_rsem.at[1, far])

    for part in range(2):
        pbuf[part] = dot(acts[0], wbuf[part, 0:kh, :]) + dot(acts[1], wbuf[part, kh:kz, :])

    chains = ((1, 0, 0), (-1, 1, 0), (1, 1, 1), (-1, 0, 1))

    def part_rows(part, zz):
        return pbuf[part, pl.ds((zz % nz) * rows, rows), :]

    for s in range(half_z):
        for n in (0, 1, 2, 3) if s == 0 else (2, 3, 0, 1):
            d, part, first = chains[n]
            if s < first:
                continue
            value = part_rows(part, z + nz + d * (half_z - s))
            if s > first:
                arrived(rs_recv.at[n, s - 1], rs_ssem.at[n, s], rs_rsem.at[n, s - 1])
                value = value + rs_recv[n, s - 1].astype(F32)
            rs_send[n, s] = value.astype(BF16)
            send(
                rs_send.at[n, s],
                rs_recv.at[n, s],
                rs_ssem.at[n, s],
                rs_rsem.at[n, s],
                epid(z + d + nz, x),
                tp,
            )
    last = half_z - 1
    for n in range(4):
        arrived(rs_recv.at[n, last], rs_ssem.at[n, last], rs_rsem.at[n, last])
    proj_x = part_rows(0, z) + rs_recv[0, last].astype(F32) + rs_recv[3, last].astype(F32)
    proj_y = part_rows(1, z) + rs_recv[1, last].astype(F32) + rs_recv[2, last].astype(F32)

    moved = proj_x.astype(BF16)
    moved_out[...] = moved
    conv = (hist[...] + moved.astype(F32) * tap[...].astype(F32)).astype(BF16)
    blocks, bw = rate_w.shape[0], rate_w.shape[1]
    rate = jnp.concatenate(
        [dot(conv[:, b * bw : (b + 1) * bw], rate_w[b]) for b in range(blocks)], axis=1
    )
    in_gate = jnp.concatenate(
        [dot(conv[:, b * bw : (b + 1) * bw], input_w[b]) for b in range(blocks)], axis=1
    )
    rate = jax.nn.sigmoid(rate)
    in_gate = jax.nn.sigmoid(in_gate)
    param = rate_param[...]
    soft = jnp.maximum(-param, 0.0) + jnp.log1p(jnp.exp(-jnp.abs(param)))
    log_decay = -8.0 * rate * soft
    tanh_decay = jnp.tanh(log_decay)
    rest = -2.0 * tanh_decay / (1.0 - tanh_decay)
    state = jnp.exp(log_decay) * state_in[...] + jnp.sqrt(rest) * in_gate * conv.astype(F32)
    state_out[...] = state
    gelu = 0.5 * proj_y * (
        1.0 + jnp.tanh(0.7978845608028654 * (proj_y + 0.044715 * proj_y * proj_y * proj_y))
    )
    gated = (state * gelu).astype(BF16)

    load_ow.wait()

    def out_cols(yy, cc):
        return pl.ds(pl.multiple_of(tpid(yy, cc) * chan, chan), chan)

    for i in (2, 1, 3, 0):
        yy = (y + i) % NY
        os_send[i] = dot(gated, out_w[:, out_cols(yy, other)]).astype(BF16)
        send(os_send.at[i], os_recv.at[i], os_ssem.at[i], os_rsem.at[i], ep, partner)
    for i in (2, 1, 3):
        yy = (y + i) % NY
        value = dot(gated, out_w[:, out_cols(yy, c)])
        arrived(os_recv.at[i], os_ssem.at[i], os_rsem.at[i])
        oy_send[i] = (value + os_recv[i].astype(F32)).astype(BF16)
        send(oy_send.at[i], oy_recv.at[i], oy_ssem.at[i], oy_rsem.at[i], ep, tpid(yy, c))
    mixed = tokens[:, out_cols(y, c)].astype(F32) + dot(gated, out_w[:, out_cols(y, c)])

    lanes = lax.broadcasted_iota(jnp.int32, (rows, ep_n), 1)
    one0 = (routes[:, 0:1] == lanes).astype(F32)
    one1 = (routes[:, 1:2] == lanes).astype(F32)
    lower = (
        lax.broadcasted_iota(jnp.int32, (rows, rows), 0)
        > lax.broadcasted_iota(jnp.int32, (rows, rows), 1)
    ).astype(F32)
    before = dot(lower.astype(BF16), (one0 + one1).astype(BF16))
    ids = lax.broadcasted_iota(jnp.int32, (rows, 2 * slots), 1).astype(F32)

    def one_hot(k, one):
        slot = jnp.sum(before * one, axis=1, keepdims=True)
        first = routes[:, k : k + 1].astype(F32) * (2.0 * cap) + slot
        return (ids == first).astype(F32), (ids == first + cap).astype(F32)

    lo0, hi0 = one_hot(0, one0)
    lo1, hi1 = one_hot(1, one1)
    lo_all = (lo0 + lo1).astype(BF16)
    hi_all = (hi0 + hi1).astype(BF16)

    arrived(os_recv.at[0], os_ssem.at[0], os_rsem.at[0])
    mixed = mixed + os_recv[0].astype(F32)
    for i in (1, 3, 2):
        arrived(oy_recv.at[i], oy_ssem.at[i], oy_rsem.at[i])
        mixed = mixed + oy_recv[i].astype(F32)
    mixed16 = mixed.astype(BF16)

    sd[...] = (dot_t(lo_all, mixed16[:, 0:ch]) + dot_t(hi_all, mixed16[:, ch:chan])).astype(BF16)
    tile = 2 * cap

    def slot_rows(e):
        return pl.ds(pl.multiple_of(e * tile, tile), tile)

    def scatter(src, dst_of, ssem, rsem):
        @pl.loop(1, ep_n)
        def _(i):
            e = (ep + i) % ep_n
            pltpu.make_async_remote_copy(
                src_ref=src.at[slot_rows(e), :],
                dst_ref=dst_of(ep),
                send_sem=ssem.at[i],
                recv_sem=rsem.at[ep],
                device_id=(e, tp),
                device_id_type=MESH,
            ).start()

    def gathered(src, dst_of, ssem, rsem):
        @pl.loop(1, ep_n)
        def _(i):
            e = (ep + i) % ep_n
            copy = pltpu.make_async_remote_copy(
                src_ref=src.at[slot_rows(e), :],
                dst_ref=dst_of(e),
                send_sem=ssem.at[i],
                recv_sem=rsem.at[e],
                device_id=(e, tp),
                device_id_type=MESH,
            )
            copy.wait_send()
            copy.wait_recv()

    def own_slot(e):
        return gbuf.at[tp, slot_rows(e), :]

    scatter(sd, own_slot, s_ssem, s_rsem)
    gbuf[tp, slot_rows(ep), :] = sd[slot_rows(ep), :]
    load_eg.wait()
    load_eu.wait()
    load_ed.wait()
    gathered(sd, own_slot, s_ssem, s_rsem)

    hrows = slots

    def half(t, h):
        return gbuf.at[t, pl.ds(h * hrows, hrows), :]

    counter = [0]

    def share(t, h, to_tp):
        send(half(t, h), half(t, h), ag_ssem.at[counter[0]], ag_rsem.at[t, h], ep, to_tp)
        counter[0] += 1

    def shared(t, h):
        arrived(half(t, h), ag_ssem.at[0], ag_rsem.at[t, h])

    up_tp = tpid(y + 1, c)
    down_tp = tpid(y + 3, c)
    far_tp = tpid(y + 2, c)
    share(tp, 0, up_tp)
    share(tp, 1, down_tp)
    share(tp, 1, up_tp)
    share(tp, 0, down_tp)
    share(tp, 0, partner)
    share(tp, 1, partner)

    squares = jnp.zeros((slots, 1), F32)

    def absorb(t, squares, first):
        value = gbuf[t].astype(F32).reshape(ep_n, 2 * cap, ch)
        parts = (value[:, 0:cap, :], value[:, cap:, :])
        for k in range(2):
            piece = parts[k].reshape(slots, ch)
            squares = squares + jnp.sum(piece * piece, axis=1, keepdims=True)
            at = pl.multiple_of(t * chan + k * ch, ch)
            piece = (piece * moe_gain[:, pl.ds(at, ch)].astype(F32)).astype(BF16)
            product = dot(piece, wgu[pl.ds(at, ch), :])
            if first and k == 0:
                acc[...] = product
            else:
                acc[...] += product
        return squares

    squares = absorb(tp, squares, True)
    shared(partner, 0)
    shared(partner, 1)
    squares = absorb(partner, squares, False)
    shared(down_tp, 0)
    share(down_tp, 0, up_tp)
    share(down_tp, 0, partner)
    shared(up_tp, 1)
    share(up_tp, 1, down_tp)
    share(up_tp, 1, partner)
    shared(down_tp, 1)
    share(down_tp, 1, partner)
    shared(up_tp, 0)
    share(up_tp, 0, partner)
    squares = absorb(down_tp, squares, False)
    squares = absorb(up_tp, squares, False)
    shared(far_tp, 0)
    share(far_tp, 0, partner)
    shared(far_tp, 1)
    share(far_tp, 1, partner)
    for i in (3, 1):
        t = tpid(y + i, other)
        shared(t, 0)
        shared(t, 1)
        squares = absorb(t, squares, False)
    squares = absorb(far_tp, squares, False)
    t = tpid(y + 2, other)
    shared(t, 0)
    shared(t, 1)
    squares = absorb(t, squares, False)

    scale2 = lax.rsqrt(squares * (1.0 / width) + 1e-06)
    gate_part = acc[:, 0:ff] * scale2
    up_part = acc[:, ff:] * scale2
    hidden = (gate_part * jax.nn.sigmoid(gate_part) * up_part).astype(BF16)

    for i in (2, 1, 3, 0):
        d_send[i] = dot(hidden, wd[:, out_cols(y + i, other)]).astype(BF16)
        send(d_send.at[i], d_recv.at[i], d_ssem.at[i], d_rsem.at[i], ep, partner)

    hs = slots // 2

    def own_part(i):
        value = dot(hidden, wd[:, out_cols(y + i, c)])
        arrived(d_recv.at[i], d_ssem.at[i], d_rsem.at[i])
        return value + d_recv[i].astype(F32)

    value = own_part(2)
    q_send[0] = value[0:hs].astype(BF16)
    send(q_send.at[0], fw_recv.at[0], q_ssem.at[0], fw_rsem.at[0], ep, up_tp)
    q_send[1] = value[hs:].astype(BF16)
    send(q_send.at[1], fw_recv.at[1], q_ssem.at[1], fw_rsem.at[1], ep, down_tp)
    value = own_part(1)
    q_send[2] = value[hs:].astype(BF16)
    send(q_send.at[2], fin_recv.at[0, 1], q_ssem.at[2], fin_rsem.at[0, 1], ep, up_tp)
    qf[0] = value[0:hs]
    value = own_part(3)
    q_send[3] = value[0:hs].astype(BF16)
    send(q_send.at[3], fin_recv.at[1, 0], q_ssem.at[3], fin_rsem.at[1, 0], ep, down_tp)
    qf[1] = value[hs:]
    arrived(fw_recv.at[0], q_ssem.at[0], fw_rsem.at[0])
    q_send[4] = (qf[0] + fw_recv[0].astype(F32)).astype(BF16)
    send(q_send.at[4], fin_recv.at[0, 0], q_ssem.at[4], fin_rsem.at[0, 0], ep, up_tp)
    arrived(fw_recv.at[1], q_ssem.at[0], fw_rsem.at[1])
    q_send[5] = (qf[1] + fw_recv[1].astype(F32)).astype(BF16)
    send(q_send.at[5], fin_recv.at[1, 1], q_ssem.at[5], fin_rsem.at[1, 1], ep, down_tp)
    value = own_part(0)
    for h in range(2):
        total = value[h * hs : (h + 1) * hs]
        for d in range(2):
            arrived(fin_recv.at[d, h], q_ssem.at[0], fin_rsem.at[d, h])
            total = total + fin_recv[d, h].astype(F32)
        total = total.reshape(hs // cap, cap, chan)
        total = jnp.concatenate([total[:, :, 0:ch], total[:, :, ch:]], axis=1)
        back_send[h * slots : (h + 1) * slots, :] = total.reshape(slots, ch).astype(BF16)

    def back_slot(e):
        return back_recv.at[slot_rows(e), :]

    scatter(back_send, back_slot, b_ssem, b_rsem)
    back_recv[slot_rows(ep), :] = back_send[slot_rows(ep), :]
    p0 = prob[:, 0:1]
    p1 = prob[:, 1:2]
    inv = 1.0 / (p0 + p1)
    gathered(back_send, back_slot, b_ssem, b_rsem)
    returned = back_recv[...]
    w0 = p0 * inv
    w1 = p1 * inv
    for k, (a, b) in enumerate(((lo0, lo1), (hi0, hi1))):
        picked = w0 * dot(a.astype(BF16), returned) + w1 * dot(b.astype(BF16), returned)
        layer_out[:, k * ch : (k + 1) * ch] = (
            mixed[:, k * ch : (k + 1) * ch] + picked
        ).astype(BF16)

    for copy in started:
        copy.wait_send()


def shards(
    tokens,
    state_in,
    conv_in,
    mix_gain,
    rnn_weight,
    gate_weight,
    conv_weight,
    rate_weight,
    input_weight,
    rate_param,
    out_weight,
    moe_gain,
    expert_gate,
    expert_up,
    expert_down,
    routes,
    route_prob,
):
    rows, width = tokens.shape
    ks, chan = rnn_weight.shape
    ep_n = lax.axis_size("ep")
    tp_n = lax.axis_size("tp")
    nz = ep_n // NX
    half_z = nz // 2
    kh = width // nz // 2
    ff = expert_down.shape[1]
    topk = routes.shape[1]
    cap = max(2, 2 * rows * topk // ep_n)
    slots = ep_n * cap
    ch = chan // 2

    taps = conv_weight.astype(F32)
    history = conv_in.astype(F32)
    hist = history[:, 0] * taps[0] + history[:, 1] * taps[1] + history[:, 2] * taps[2]

    vm = pl.BlockSpec(memory_space=pltpu.VMEM)
    hbm = pl.BlockSpec(memory_space=pl.ANY)
    dma = pltpu.SemaphoreType.DMA
    layer_out, state_out, moved = pl.pallas_call(
        layer_kernel,
        out_shape=(
            jax.ShapeDtypeStruct((rows, chan), BF16),
            jax.ShapeDtypeStruct((rows, chan), F32),
            jax.ShapeDtypeStruct((rows, chan), BF16),
        ),
        in_specs=[vm] * 13 + [hbm] * 4,
        out_specs=(vm, vm, vm),
        scratch_shapes=[
            pltpu.VMEM((chan, width), BF16),
            pltpu.VMEM((width, 2 * ff), BF16),
            pltpu.VMEM((ff, width), BF16),
            pltpu.VMEM((2 * nz, rows, kh), BF16),
            pltpu.VMEM((2, nz * rows, kh), BF16),
            pltpu.VMEM((2, NX * ks, chan), BF16),
            pltpu.VMEM((2, nz * rows, chan), F32),
            pltpu.VMEM((4, half_z, rows, chan), BF16),
            pltpu.VMEM((4, half_z, rows, chan), BF16),
            pltpu.VMEM((NY, rows, chan), BF16),
            pltpu.VMEM((NY, rows, chan), BF16),
            pltpu.VMEM((NY, rows, chan), BF16),
            pltpu.VMEM((NY, rows, chan), BF16),
            pltpu.VMEM((2 * slots, ch), BF16),
            pltpu.VMEM((tp_n, 2 * slots, ch), BF16),
            pltpu.VMEM((16, 128), BF16),
            pltpu.VMEM((slots, 2 * ff), F32),
            pltpu.VMEM((NY, slots, chan), BF16),
            pltpu.VMEM((NY, slots, chan), BF16),
            pltpu.VMEM((2, slots // 2, chan), F32),
            pltpu.VMEM((6, slots // 2, chan), BF16),
            pltpu.VMEM((2, slots // 2, chan), BF16),
            pltpu.VMEM((2, 2, slots // 2, chan), BF16),
            pltpu.VMEM((2 * slots, ch), BF16),
            pltpu.VMEM((2 * slots, ch), BF16),
            dma((4,)),
            dma((6,)),
            dma((2, NX)),
            dma((nz,)),
            dma((nz,)),
            dma((nz,)),
            dma((nz,)),
            dma((4, half_z)),
            dma((4, half_z)),
            dma((NY,)),
            dma((NY,)),
            dma((NY,)),
            dma((NY,)),
            dma((ep_n,)),
            dma((ep_n,)),
            dma((14,)),
            dma((tp_n, 2)),
            dma((NY,)),
            dma((NY,)),
            dma((6,)),
            dma((2,)),
            dma((2, 2)),
            dma((ep_n,)),
            dma((ep_n,)),
        ],
        compiler_params=pltpu.CompilerParams(
            collective_id=0,
            has_side_effects=True,
            vmem_limit_bytes=60 * 1024 * 1024,
        ),
        name="layer",
    )(
        tokens,
        hist,
        state_in,
        mix_gain.reshape(1, width),
        rnn_weight,
        gate_weight,
        conv_weight[3:4],
        rate_weight,
        input_weight,
        rate_param.reshape(1, chan),
        moe_gain.reshape(1, width),
        routes,
        route_prob,
        out_weight,
        expert_gate,
        expert_up,
        expert_down,
    )
    conv_out = jnp.concatenate([conv_in[:, 1:], moved[:, None, :]], axis=1)
    return (layer_out, state_out, conv_out)


def solution(mesh):
    in_specs = (
        P("ep", None),
        P("ep", "tp"),
        P("ep", None, "tp"),
        P(),
        P("ep", "tp"),
        P("ep", "tp"),
        P(None, "tp"),
        P("tp", None, None),
        P("tp", None, None),
        P("tp"),
        P("tp", None),
        P(),
        P("ep", None, "tp"),
        P("ep", None, "tp"),
        P("ep", "tp", None),
        P("ep", None),
        P("ep", None),
    )
    out_specs = (P("ep", "tp"), P("ep", "tp"), P("ep", None, "tp"))
    return jax.shard_map(shards, mesh=mesh, in_specs=in_specs, out_specs=out_specs, check_vma=False)
```

time: 297 us -> 110 us (0.37)
  waiting for transfers between devices: 164 us -> 0 us
  Pallas kernels: 0 us -> 93.8 us
  blocking collectives: 58.8 us -> 0 us
  matrix products: 20 us -> 0 us
  between operations: 14.3 us -> 0.66 us
  other arithmetic: 15.1 us -> 3.19 us
  starting transfers between devices: 11.7 us -> 0 us
    all_gather x2 -> x0, waiting for transfers between devices: 130 us -> none  [the longest x1 97.8 us: side_by_side(): lax.all_gather(both, axis, axis=dim, tiled=True)]
    pallas_call x0 -> x1, Pallas kernels: none -> 93.8 us  [shards(): pl.pallas_call(layer_kernel, out_shape=(jax.ShapeDtypeStruct((rows, chan)...]
    all_to_all x1 -> x0, blocking collectives: 58.8 us -> none  [shards(): lax.all_to_all(send, 'ep', split_axis=0, concat_axis=0, tiled=True)]
    all_to_all x2 -> x0, waiting for transfers between devices: 33.7 us -> none  [the longest x1 26.3 us: sum_at_owner(): parts = lax.all_to_all(in_blocks(shard, dim, size), axis, 0, 0, tiled=True)]
    dot_general x8 -> x0, matrix products: 20 us -> none  [the longest x1 6.08 us: shards(): partial_out = jnp.dot(gated, out_weight, preferred_element_type=jnp.float32)]
    all_to_all x2 -> x0, starting transfers between devices: 11.7 us -> none  [the longest x1 6.35 us: sum_at_owner(): parts = lax.all_to_all(in_blocks(shard, dim, size), axis, 0, 0, tiled=True)]
    reduce_sum x6 -> x0, other arithmetic: 7.39 us -> none  [the longest x1 3.04 us: over_pieces(): return parts.sum(axis=0)]
    unnamed x25 -> x4, local copies, waits for them, and re-layouts: 1.98 us -> 5.8 us
  transfers between devices with their start and end apart: 4 -> 0, of which waited for: 4 -> 0; matrix products, arithmetic and copies ran while one was open for 3% -> 0% of each run, Pallas kernels for 0% -> 0%
where the time goes in v1:
time: 110 us; the launch traced here: 108 us
  Pallas kernels  93.8 us (85%)
  local copies, waits for them, and re-layouts  10.5 us (10%)
  other arithmetic  3.19 us (3%)
    pallas_call x1, Pallas kernels, shards(): pl.pallas_call(layer_kernel, out_shape=(jax.ShapeDtypeStruct((rows, chan)...  93.8 us
    unnamed x4, local copies, waits for them, and re-layouts  5.8 us

profile of v1, /device:TPU:1, one launch (start us, length us, event | category | flops | bytes accessed | tf_op | source)
XLA Modules:
  0.0 108.1 jit_solution(9080155220752323352)
XLA Ops:
  0.6 1.0 convert_element_type.6
  1.6 0.8 fusion.5
  2.4 0.7 fusion.1.hist
  3.1 1.3 %reshape.15.mix_gain = bf16[1,4096]{1,0:T(2,128)(2,1)} reshape(bf16[4096]{0:T(1024)(128)(2,1)} %param.20) | data formatting | bytes 16384 | tf_op jit(solution)/shard_map/reshape | solution.py:629
  4.4 1.3 %slice.30.tap = bf16[1,512]{1,0:T(2,128)(2,1)} slice(bf16[4,512]{1,0:T(4,128)(2,1)} %param.23), slice={[3:4], [0:512]} | slice | bytes 2048 | tf_op jit(solution)/shard_map/slice | solution.py:632
  5.7 1.3 %reshape.17.moe_gain = bf16[1,4096]{1,0:T(2,128)(2,1)} reshape(bf16[4096]{0:T(1024)(128)(2,1)} %param.28) | data formatting | bytes 16384 | tf_op jit(solution)/shard_map/reshape | solution.py:636
  7.0 1.4 %copy.20.routes = s32[64,2]{1,0:T(8,128)} copy(s32[64,2]{0,1:T(2,128)} %param.32) | data formatting | bytes 1024 | tf_op args[15]
  8.3 1.4 %copy.21.prob = f32[64,2]{1,0:T(8,128)} copy(f32[64,2]{0,1:T(2,128)} %param.33) | data formatting | bytes 1024 | tf_op args[16]
  9.7 0.0 slice-start
  9.7 93.8 %layer.1 = (bf16[64,512]{1,0:T(8,128)(2,1)}, f32[64,512]{1,0:T(8,128)}, bf16[64,512]{1,0:T(8,128)(2,1)}) custom-call(bf16[64,4096]{1,0:T(8,128)(2,1)} %tokens.1, f32[64,512]{1,0:T(8,128)} %fusion.1.hist, f32[64,512]{1,0:T(8,128)} %state_in.1, bf16[1,4096]{1,0:T(2,128)(2,1)} %reshape.15.mix_gain, bf16[128,512]{1,0:T(8,128)(2,1)} %rnn_w.1, ...), custom_call_target="tpu_custom_call" | custom-call | tf_op jit(solution)/shard_map/layer/pallas_call | solution.py:559
  103.6 0.0 slice-done
  103.6 1.5 %pad_maximum_fusion = bf16[64,3,512]{2,0,1:T(8,128)(2,1)} fusion(bf16[64,1,512]{2,0,1:T(8,128)(2,1)} %bitcast.25, bf16[64,2,512]{2,0,1:T(8,128)(2,1)S(1)} %slice-done), kind=kLoop, calls=%fused_computation | loop fusion | flops 98304 | bytes 393216 | tf_op jit(solution)/shard_map/concatenate | solution.py:644
  105.1 1.5 %copy.24 = bf16[64,512]{1,0:T(8,128)(2,1)} copy(bf16[64,512]{1,0:T(8,128)(2,1)} %get-tuple-element.15) | data formatting | bytes 131072
  106.6 1.6 %copy.25 = f32[64,512]{1,0:T(8,128)} copy(f32[64,512]{1,0:T(8,128)} %get-tuple-element.16) | data formatting | bytes 262144
Async XLA Ops:
  9.7 93.8 %slice-start = ((bf16[64,3,512]{2,0,1:T(8,128)(2,1)}), bf16[64,2,512]{2,0,1:T(8,128)(2,1)S(1)}, s32[]{:S(2)}) async-start(bf16[64,3,512]{2,0,1:T(8,128)(2,1)} %param.19), calls=%async_computation | async-start | bytes 262144 | tf_op jit(solution)/shard_map/slice | solution.py:644

commit v2 on v1

--- a/solution.py
+++ b/solution.py
@@ -23,14 +23,26 @@
     return lax.dot_general(a, b, (((0,), (0,)), ((), ())), preferred_element_type=F32)
 
 
+class Phases:
+    def __init__(self):
+        self.scope = None
+
+    def __call__(self, name):
+        if self.scope is not None:
+            self.scope.__exit__(None, None, None)
+        self.scope = jax.named_scope(name) if name else None
+        if self.scope is not None:
+            self.scope.__enter__()
+
+
 def layer_kernel(
     tokens,
-    hist,
+    conv_in,
     state_in,
     mix_gain,
     rnn_w,
     gate_w,
-    tap,
+    taps,
     rate_w,
     input_w,
     rate_param,
@@ -43,7 +55,7 @@
     ed_hbm,
     layer_out,
     state_out,
-    moved_out,
+    conv_out,
     out_w,
     wgu,
     wd,
@@ -59,7 +71,7 @@
     oy_recv,
     sd,
     gbuf,
-    xg,
+    gain2,
     acc,
     d_send,
     d_recv,
@@ -147,6 +159,8 @@
             device_id_type=MESH,
         ).wait_recv()
 
+    phase = Phases()
+    phase("start")
     load_ow = pltpu.make_async_copy(out_w_hbm, out_w, local_sem.at[0])
     load_eg = pltpu.make_async_copy(eg_hbm.at[0], wgu.at[:, pl.ds(0, ff)], local_sem.at[1])
     load_eu = pltpu.make_async_copy(eu_hbm.at[0], wgu.at[:, pl.ds(ff, ff)], local_sem.at[2])
@@ -172,15 +186,20 @@
 
     base = tokens[...].astype(F32)
     scale = lax.rsqrt(jnp.mean(base * base, axis=-1, keepdims=True) + 1e-06)
-    normed = (base * scale * mix_gain[...].astype(F32)).astype(BF16)
-    for k in range(2 * nz):
-        nrm[k] = normed[:, k * kh : (k + 1) * kh]
+    gain = mix_gain[...].astype(F32)
+    gain2[...] = moe_gain[...].astype(F32)
+    for k in range(width // 128):
+        piece = base[:, k * 128 : (k + 1) * 128] * scale * gain[k : k + 1, :]
+        at = k * 128 % kh
+        nrm[k * 128 // kh, :, at : at + 128] = piece.astype(BF16)
     wbuf[0, pl.ds(x * ks, ks), :] = rnn_w[...]
     wbuf[1, pl.ds(x * ks, ks), :] = gate_w[...]
     for h in range(2):
         acts[h, pl.ds(z * rows, rows), :] = nrm[2 * z + h]
 
+    phase("barrier")
     pl.semaphore_wait(barrier, ep_n - 1 + tp_n - 1)
+    phase("acts")
 
     own_w = (rnn_w, gate_w)
 
@@ -218,6 +237,7 @@
         arrived(block, a_ssem.at[i], a_rsem.at[from_z])
         send(block, block, ad_ssem.at[i], ad_rsem.at[from_z], ep, partner)
 
+    phase("weights")
     left = (x + NX - 1) % NX
     right = (x + 1) % NX
     far = (x + 2) % NX
@@ -234,9 +254,17 @@
     arrived(w_slot(0, far), w_ssem.at[0], w_rsem.at[0, far])
     arrived(w_slot(1, far), w_ssem.at[0], w_rsem.at[1, far])
 
+    phase("proj")
     for part in range(2):
         pbuf[part] = dot(acts[0], wbuf[part, 0:kh, :]) + dot(acts[1], wbuf[part, kh:kz, :])
 
+    tap = taps[...].astype(F32)
+    hist = conv_in[0].astype(F32) * tap[0:1]
+    for i in (1, 2):
+        conv_out[i - 1] = conv_in[i]
+        hist = hist + conv_in[i].astype(F32) * tap[i : i + 1]
+
+    phase("zring")
     chains = ((1, 0, 0), (-1, 1, 0), (1, 1, 1), (-1, 0, 1))
 
     def part_rows(part, zz):
@@ -266,9 +294,10 @@
     proj_x = part_rows(0, z) + rs_recv[0, last].astype(F32) + rs_recv[3, last].astype(F32)
     proj_y = part_rows(1, z) + rs_recv[1, last].astype(F32) + rs_recv[2, last].astype(F32)
 
+    phase("recur")
     moved = proj_x.astype(BF16)
-    moved_out[...] = moved
-    conv = (hist[...] + moved.astype(F32) * tap[...].astype(F32)).astype(BF16)
+    conv_out[2] = moved
+    conv = (hist + moved.astype(F32) * tap[3:4]).astype(BF16)
     blocks, bw = rate_w.shape[0], rate_w.shape[1]
     rate = jnp.concatenate(
         [dot(conv[:, b * bw : (b + 1) * bw], rate_w[b]) for b in range(blocks)], axis=1
@@ -290,6 +319,7 @@
     )
     gated = (state * gelu).astype(BF16)
 
+    phase("outproj")
     load_ow.wait()
 
     def out_cols(yy, cc):
@@ -307,19 +337,19 @@
         send(oy_send.at[i], oy_recv.at[i], oy_ssem.at[i], oy_rsem.at[i], ep, tpid(yy, c))
     mixed = tokens[:, out_cols(y, c)].astype(F32) + dot(gated, out_w[:, out_cols(y, c)])
 
-    lanes = lax.broadcasted_iota(jnp.int32, (rows, ep_n), 1)
-    one0 = (routes[:, 0:1] == lanes).astype(F32)
-    one1 = (routes[:, 1:2] == lanes).astype(F32)
-    lower = (
-        lax.broadcasted_iota(jnp.int32, (rows, rows), 0)
-        > lax.broadcasted_iota(jnp.int32, (rows, rows), 1)
-    ).astype(F32)
-    before = dot(lower.astype(BF16), (one0 + one1).astype(BF16))
-    ids = lax.broadcasted_iota(jnp.int32, (rows, 2 * slots), 1).astype(F32)
+    phase("slots")
+    experts = lax.broadcasted_iota(jnp.int32, (ep_n, rows), 0)
+    one0 = (routes[0:1, :] == experts).astype(F32)
+    one1 = (routes[1:2, :] == experts).astype(F32)
+    row_ids = lax.broadcasted_iota(jnp.int32, (rows, rows), 0)
+    col_ids = lax.broadcasted_iota(jnp.int32, (rows, rows), 1)
+    upper = (row_ids < col_ids).astype(F32).astype(BF16)
+    before = dot((one0 + one1).astype(BF16), upper)
+    ids = lax.broadcasted_iota(jnp.int32, (2 * slots, rows), 0).astype(F32)
 
     def one_hot(k, one):
-        slot = jnp.sum(before * one, axis=1, keepdims=True)
-        first = routes[:, k : k + 1].astype(F32) * (2.0 * cap) + slot
+        slot = jnp.sum(before * one, axis=0, keepdims=True)
+        first = routes[k : k + 1, :].astype(F32) * (2.0 * cap) + slot
         return (ids == first).astype(F32), (ids == first + cap).astype(F32)
 
     lo0, hi0 = one_hot(0, one0)
@@ -327,6 +357,7 @@
     lo_all = (lo0 + lo1).astype(BF16)
     hi_all = (hi0 + hi1).astype(BF16)
 
+    phase("mixwait")
     arrived(os_recv.at[0], os_ssem.at[0], os_rsem.at[0])
     mixed = mixed + os_recv[0].astype(F32)
     for i in (1, 3, 2):
@@ -334,7 +365,8 @@
         mixed = mixed + oy_recv[i].astype(F32)
     mixed16 = mixed.astype(BF16)
 
-    sd[...] = (dot_t(lo_all, mixed16[:, 0:ch]) + dot_t(hi_all, mixed16[:, ch:chan])).astype(BF16)
+    phase("dispatch")
+    sd[...] = (dot(lo_all, mixed16[:, 0:ch]) + dot(hi_all, mixed16[:, ch:chan])).astype(BF16)
     tile = 2 * cap
 
     def slot_rows(e):
@@ -373,10 +405,13 @@
 
     scatter(sd, own_slot, s_ssem, s_rsem)
     gbuf[tp, slot_rows(ep), :] = sd[slot_rows(ep), :]
+    phase("loadwait")
     load_eg.wait()
     load_eu.wait()
     load_ed.wait()
+    phase("a2a_wait")
     gathered(sd, own_slot, s_ssem, s_rsem)
+    phase("ag_own")
 
     hrows = slots
 
@@ -411,8 +446,11 @@
             piece = parts[k].reshape(slots, ch)
             squares = squares + jnp.sum(piece * piece, axis=1, keepdims=True)
             at = pl.multiple_of(t * chan + k * ch, ch)
-            piece = (piece * moe_gain[:, pl.ds(at, ch)].astype(F32)).astype(BF16)
-            product = dot(piece, wgu[pl.ds(at, ch), :])
+            lanes = []
+            for j in range(ch // 128):
+                g = gain2[pl.ds(t * (chan // 128) + (k * ch) // 128 + j, 1), :]
+                lanes.append((piece[:, j * 128 : (j + 1) * 128] * g).astype(BF16))
+            product = dot(jnp.concatenate(lanes, axis=1), wgu[pl.ds(at, ch), :])
             if first and k == 0:
                 acc[...] = product
             else:
@@ -420,9 +458,11 @@
         return squares
 
     squares = absorb(tp, squares, True)
+    phase("ag_partner")
     shared(partner, 0)
     shared(partner, 1)
     squares = absorb(partner, squares, False)
+    phase("ag_near")
     shared(down_tp, 0)
     share(down_tp, 0, up_tp)
     share(down_tp, 0, partner)
@@ -433,28 +473,34 @@
     share(down_tp, 1, partner)
     shared(up_tp, 0)
     share(up_tp, 0, partner)
+    phase("absorb_near")
     squares = absorb(down_tp, squares, False)
     squares = absorb(up_tp, squares, False)
+    phase("ag_far")
     shared(far_tp, 0)
     share(far_tp, 0, partner)
     shared(far_tp, 1)
     share(far_tp, 1, partner)
+    phase("ag_other")
     for i in (3, 1):
         t = tpid(y + i, other)
         shared(t, 0)
         shared(t, 1)
         squares = absorb(t, squares, False)
+    phase("ag_last")
     squares = absorb(far_tp, squares, False)
     t = tpid(y + 2, other)
     shared(t, 0)
     shared(t, 1)
     squares = absorb(t, squares, False)
 
+    phase("hidden")
     scale2 = lax.rsqrt(squares * (1.0 / width) + 1e-06)
     gate_part = acc[:, 0:ff] * scale2
     up_part = acc[:, ff:] * scale2
     hidden = (gate_part * jax.nn.sigmoid(gate_part) * up_part).astype(BF16)
 
+    phase("down_send")
     for i in (2, 1, 3, 0):
         d_send[i] = dot(hidden, wd[:, out_cols(y + i, other)]).astype(BF16)
         send(d_send.at[i], d_recv.at[i], d_ssem.at[i], d_rsem.at[i], ep, partner)
@@ -466,6 +512,7 @@
         arrived(d_recv.at[i], d_ssem.at[i], d_rsem.at[i])
         return value + d_recv[i].astype(F32)
 
+    phase("down_own")
     value = own_part(2)
     q_send[0] = value[0:hs].astype(BF16)
     send(q_send.at[0], fw_recv.at[0], q_ssem.at[0], fw_rsem.at[0], ep, up_tp)
@@ -479,12 +526,14 @@
     q_send[3] = value[0:hs].astype(BF16)
     send(q_send.at[3], fin_recv.at[1, 0], q_ssem.at[3], fin_rsem.at[1, 0], ep, down_tp)
     qf[1] = value[hs:]
+    phase("rs_fw")
     arrived(fw_recv.at[0], q_ssem.at[0], fw_rsem.at[0])
     q_send[4] = (qf[0] + fw_recv[0].astype(F32)).astype(BF16)
     send(q_send.at[4], fin_recv.at[0, 0], q_ssem.at[4], fin_rsem.at[0, 0], ep, up_tp)
     arrived(fw_recv.at[1], q_ssem.at[0], fw_rsem.at[1])
     q_send[5] = (qf[1] + fw_recv[1].astype(F32)).astype(BF16)
     send(q_send.at[5], fin_recv.at[1, 1], q_ssem.at[5], fin_rsem.at[1, 1], ep, down_tp)
+    phase("rs_fin")
     value = own_part(0)
     for h in range(2):
         total = value[h * hs : (h + 1) * hs]
@@ -495,26 +544,34 @@
         total = jnp.concatenate([total[:, :, 0:ch], total[:, :, ch:]], axis=1)
         back_send[h * slots : (h + 1) * slots, :] = total.reshape(slots, ch).astype(BF16)
 
+    phase("back")
     def back_slot(e):
         return back_recv.at[slot_rows(e), :]
 
     scatter(back_send, back_slot, b_ssem, b_rsem)
     back_recv[slot_rows(ep), :] = back_send[slot_rows(ep), :]
-    p0 = prob[:, 0:1]
-    p1 = prob[:, 1:2]
-    inv = 1.0 / (p0 + p1)
+    total = prob[0:1, :] + prob[1:2, :]
+    eye = row_ids == col_ids
+
+    def column(row):
+        return jnp.sum(jnp.where(eye, row, 0.0), axis=1, keepdims=True)
+
+    w0 = column(prob[0:1, :] / total)
+    w1 = column(prob[1:2, :] / total)
+    phase("back_wait")
     gathered(back_send, back_slot, b_ssem, b_rsem)
+    phase("combine")
     returned = back_recv[...]
-    w0 = p0 * inv
-    w1 = p1 * inv
     for k, (a, b) in enumerate(((lo0, lo1), (hi0, hi1))):
-        picked = w0 * dot(a.astype(BF16), returned) + w1 * dot(b.astype(BF16), returned)
+        picked = w0 * dot_t(a.astype(BF16), returned) + w1 * dot_t(b.astype(BF16), returned)
         layer_out[:, k * ch : (k + 1) * ch] = (
             mixed[:, k * ch : (k + 1) * ch] + picked
         ).astype(BF16)
 
+    phase("drain")
     for copy in started:
         copy.wait_send()
+    phase(None)
 
 
 def shards(
@@ -549,19 +606,15 @@
     slots = ep_n * cap
     ch = chan // 2
 
-    taps = conv_weight.astype(F32)
-    history = conv_in.astype(F32)
-    hist = history[:, 0] * taps[0] + history[:, 1] * taps[1] + history[:, 2] * taps[2]
-
     vm = pl.BlockSpec(memory_space=pltpu.VMEM)
     hbm = pl.BlockSpec(memory_space=pl.ANY)
     dma = pltpu.SemaphoreType.DMA
-    layer_out, state_out, moved = pl.pallas_call(
+    layer_out, state_out, conv_out = pl.pallas_call(
         layer_kernel,
         out_shape=(
             jax.ShapeDtypeStruct((rows, chan), BF16),
             jax.ShapeDtypeStruct((rows, chan), F32),
-            jax.ShapeDtypeStruct((rows, chan), BF16),
+            jax.ShapeDtypeStruct((3, rows, chan), BF16),
         ),
         in_specs=[vm] * 13 + [hbm] * 4,
         out_specs=(vm, vm, vm),
@@ -581,7 +634,7 @@
             pltpu.VMEM((NY, rows, chan), BF16),
             pltpu.VMEM((2 * slots, ch), BF16),
             pltpu.VMEM((tp_n, 2 * slots, ch), BF16),
-            pltpu.VMEM((16, 128), BF16),
+            pltpu.VMEM((width // 128, 128), F32),
             pltpu.VMEM((slots, 2 * ff), F32),
             pltpu.VMEM((NY, slots, chan), BF16),
             pltpu.VMEM((NY, slots, chan), BF16),
@@ -624,25 +677,24 @@
         name="layer",
     )(
         tokens,
-        hist,
+        conv_in.transpose(1, 0, 2),
         state_in,
-        mix_gain.reshape(1, width),
+        mix_gain.reshape(width // 128, 128),
         rnn_weight,
         gate_weight,
-        conv_weight[3:4],
+        conv_weight,
         rate_weight,
         input_weight,
         rate_param.reshape(1, chan),
-        moe_gain.reshape(1, width),
-        routes,
-        route_prob,
+        moe_gain.reshape(width // 128, 128),
+        routes.T,
+        route_prob.T,
         out_weight,
         expert_gate,
         expert_up,
         expert_down,
     )
-    conv_out = jnp.concatenate([conv_in[:, 1:], moved[:, None, :]], axis=1)
-    return (layer_out, state_out, conv_out)
+    return (layer_out, state_out, conv_out.transpose(1, 0, 2))
 
 
 def solution(mesh):

time: 110 us -> 101 us (0.918)
  local copies, waits for them, and re-layouts: 10.5 us -> 4.66 us
  other arithmetic: 3.19 us -> 0 us
    reshape x2 -> x0, local copies, waits for them, and re-layouts: 2.61 us -> none  [the longest x1 1.3 us: shards(): mix_gain.reshape(1, width)]
    slice x4 -> x0, local copies, waits for them, and re-layouts: 2.06 us -> none  [the longest x1 1.25 us: shards(): conv_weight[3:4]]
    concatenate x1 -> x0, other arithmetic: 1.54 us -> none  [shards(): conv_out = jnp.concatenate([conv_in[:, 1:], moved[:, None, :]], axis=1)]
    unnamed x4 -> x3, local copies, waits for them, and re-layouts: 5.8 us -> 4.66 us
where the time goes in v2:
time: 101 us; the launch traced here: 99.2 us
  Pallas kernels  93.9 us (93%)
  local copies, waits for them, and re-layouts  4.66 us (5%)
    pallas_call x1, Pallas kernels, shards(): pl.pallas_call(layer_kernel, out_shape=(jax.ShapeDtypeStruct((rows, chan)...  93.9 us
    unnamed x3, local copies, waits for them, and re-layouts  4.66 us

profile of v2, /device:TPU:1, one launch (start us, length us, event | category | flops | bytes accessed | tf_op | source)
XLA Modules:
  0.0 99.2 jit_solution(3887986249753216641)
XLA Ops:
  0.6 93.9 %layer.1 = (bf16[64,512]{1,0:T(8,128)(2,1)}, f32[64,512]{1,0:T(8,128)}, bf16[3,64,512]{2,1,0:T(8,128)(2,1)}) custom-call(bf16[64,4096]{1,0:T(8,128)(2,1)} %tokens.1, bf16[3,64,512]{2,1,0:T(8,128)(2,1)} %bitcast.8, f32[64,512]{1,0:T(8,128)} %state_in.1, bf16[32,128]{1,0:T(8,128)(2,1)} %bitcast.9, bf16[128,512]{1,0:T(8,128)(2,1)} %rnn_w.1, ...), custom_call_target="tpu_custom_call" | custom-call | tf_op jit(solution)/shard_map/layer/pallas_call | solution.py:612
  94.6 1.5 %copy.23 = bf16[64,512]{1,0:T(8,128)(2,1)} copy(bf16[64,512]{1,0:T(8,128)(2,1)} %get-tuple-element.12) | data formatting | bytes 131072
  96.1 1.6 %copy.24 = f32[64,512]{1,0:T(8,128)} copy(f32[64,512]{1,0:T(8,128)} %get-tuple-element.13) | data formatting | bytes 262144
  97.6 1.6 %copy.25 = bf16[64,3,512]{2,0,1:T(8,128)(2,1)} copy(bf16[64,3,512]{2,0,1:T(8,128)(2,1)} %bitcast.7) | data formatting | bytes 393216

commit v3 on v2

v3 whole, which is shorter than its diff:
```python
import functools

import jax
import jax.numpy as jnp
from jax import lax
from jax.experimental import pallas as pl
from jax.experimental.pallas import tpu as pltpu
from jax.sharding import PartitionSpec as P

NX = 4
NY = 4
NC = 2
MESH = pl.DeviceIdType.MESH
F32 = jnp.float32
BF16 = jnp.bfloat16


def dot(a, b):
    return jnp.dot(a, b, preferred_element_type=F32)


def dot_t(a, b):
    return lax.dot_general(a, b, (((0,), (0,)), ((), ())), preferred_element_type=F32)


class Phases:
    def __init__(self):
        self.scope = None

    def __call__(self, name):
        if self.scope is not None:
            self.scope.__exit__(None, None, None)
        self.scope = jax.named_scope(name) if name else None
        if self.scope is not None:
            self.scope.__enter__()


def layer_kernel(
    tokens_hbm,
    conv_in_hbm,
    state_in_hbm,
    mix_gain_hbm,
    rnn_w_hbm,
    gate_w_hbm,
    taps_hbm,
    rate_w_hbm,
    input_w_hbm,
    rate_param_hbm,
    moe_gain_hbm,
    routes_hbm,
    prob_hbm,
    out_w_hbm,
    eg_hbm,
    eu_hbm,
    ed_hbm,
    layer_out,
    state_out,
    conv_out,
    tokens,
    conv_in,
    state_in,
    mix_gain,
    taps,
    rate_w,
    input_w,
    rate_param,
    moe_gain,
    routes,
    prob,
    out_w,
    wgu,
    wd,
    nrm,
    acts,
    wbuf,
    pbuf,
    rs_send,
    rs_recv,
    os_send,
    os_recv,
    oy_send,
    oy_recv,
    sd,
    gbuf,
    gain2,
    acc,
    d_send,
    d_recv,
    qf,
    q_send,
    fw_recv,
    fin_recv,
    back_send,
    back_recv,
    local_sem,
    w_ssem,
    w_rsem,
    a_ssem,
    a_rsem,
    ad_ssem,
    ad_rsem,
    rs_ssem,
    rs_rsem,
    os_ssem,
    os_rsem,
    oy_ssem,
    oy_rsem,
    s_ssem,
    s_rsem,
    ag_ssem,
    ag_rsem,
    ao_rsem,
    d_ssem,
    d_rsem,
    q_ssem,
    fw_rsem,
    fin_rsem,
    b_ssem,
    b_rsem,
):
    rows, width = tokens.shape
    ks, chan = rnn_w_hbm.shape
    ep_n = width // ks
    nz = ep_n // NX
    half_z = nz // 2
    tp_n = NY * NC
    kz = width // nz
    kh = kz // 2
    ff = wd.shape[0]
    cap = sd.shape[0] // ep_n // 2
    ch = chan // 2
    slots = ep_n * cap

    ep = lax.axis_index("ep")
    tp = lax.axis_index("tp")
    z = ep // NX
    x = ep % NX
    y = tp // NC
    c = tp % NC
    other = (c + 1) % NC

    def epid(zz, xx):
        return (zz % nz) * NX + xx % NX

    def tpid(yy, cc):
        return (yy % NY) * NC + cc

    partner = tpid(y, other)

    def send(src, dst, ssem, rsem, to_ep, to_tp):
        copy = pltpu.make_async_remote_copy(
            src_ref=src,
            dst_ref=dst,
            send_sem=ssem,
            recv_sem=rsem,
            device_id=(to_ep, to_tp),
            device_id_type=MESH,
        )
        copy.start()

    def arrived(dst, ssem, rsem):
        pltpu.make_async_remote_copy(
            src_ref=dst,
            dst_ref=dst,
            send_sem=ssem,
            recv_sem=rsem,
            device_id=(ep, partner),
            device_id_type=MESH,
        ).wait_recv()

    def sent(src, ssem, rsem):
        pltpu.make_async_remote_copy(
            src_ref=src,
            dst_ref=src,
            send_sem=ssem,
            recv_sem=rsem,
            device_id=(ep, partner),
            device_id_type=MESH,
        ).wait_send()

    phase = Phases()
    phase("start")

    barrier = pltpu.get_barrier_semaphore()

    @pl.loop(1, ep_n)
    def _(i):
        pl.semaphore_signal(
            barrier, inc=1, device_id=((ep + i) % ep_n, tp), device_id_type=MESH
        )

    @pl.loop(1, tp_n)
    def _(i):
        pl.semaphore_signal(
            barrier, inc=1, device_id=(ep, (tp + i) % tp_n), device_id_type=MESH
        )

    def own_rows(part):
        return wbuf.at[part, pl.ds(x * ks, ks), :]

    loads = {}
    for n, (name, src, dst) in enumerate(
        (
            ("tokens", tokens_hbm, tokens),
            ("mix_gain", mix_gain_hbm, mix_gain),
            ("rnn_w", rnn_w_hbm, own_rows(0)),
            ("gate_w", gate_w_hbm, own_rows(1)),
            ("moe_gain", moe_gain_hbm, moe_gain),
            ("conv_in", conv_in_hbm, conv_in),
            ("taps", taps_hbm, taps),
            ("rate_w", rate_w_hbm, rate_w),
            ("input_w", input_w_hbm, input_w),
            ("rate_param", rate_param_hbm, rate_param),
            ("state_in", state_in_hbm, state_in),
            ("routes", routes_hbm, routes),
            ("prob", prob_hbm, prob),
            ("out_w", out_w_hbm, out_w),
            ("eg", eg_hbm.at[0], wgu.at[:, pl.ds(0, ff)]),
            ("eu", eu_hbm.at[0], wgu.at[:, pl.ds(ff, ff)]),
            ("ed", ed_hbm.at[0], wd),
        )
    ):
        loads[name] = pltpu.make_async_copy(src, dst, local_sem.at[n])
        loads[name].start()

    loads["tokens"].wait()
    loads["mix_gain"].wait()
    base = tokens[...].astype(F32)
    scale = lax.rsqrt(jnp.mean(base * base, axis=-1, keepdims=True) + 1e-06)
    gain = mix_gain[...].astype(F32)
    for k in range(width // 128):
        piece = base[:, k * 128 : (k + 1) * 128] * scale * gain[k : k + 1, :]
        at = k * 128 % kh
        nrm[k * 128 // kh, :, at : at + 128] = piece.astype(BF16)
    for h in range(2):
        acts[h, pl.ds(z * rows, rows), :] = nrm[2 * z + h]
    loads["rnn_w"].wait()
    loads["gate_w"].wait()

    phase("barrier")
    pl.semaphore_wait(barrier, ep_n - 1 + tp_n - 1)
    phase("acts")

    left = (x + NX - 1) % NX
    right = (x + 1) % NX
    far = (x + 2) % NX
    hk = ks // 2

    def w_slot(part, xx, h):
        return wbuf.at[part, pl.ds(xx * ks + h * hk, hk), :]

    def w_send(part, xx, h, to_x):
        slot = w_slot(part, xx, h)
        send(slot, slot, w_ssem.at[part], w_rsem.at[part, xx, h], epid(z, to_x), tp)

    def w_wait(part, xx, h):
        arrived(w_slot(part, xx, h), w_ssem.at[part], w_rsem.at[part, xx, h])

    def w_direct(part):
        w_send(part, x, 0, right)
        w_send(part, x, 1, left)
        w_send(part, x, 1, right)
        w_send(part, x, 0, left)

    def w_forward(part):
        w_wait(part, left, 0)
        w_send(part, left, 0, right)
        w_wait(part, right, 1)
        w_send(part, right, 1, left)

    def w_rest(part):
        w_wait(part, left, 1)
        w_wait(part, right, 0)
        w_wait(part, far, 0)
        w_wait(part, far, 1)

    w_direct(0)

    order = []
    for i in range(half_z, 0, -1):
        order.append(i)
        if i < half_z:
            order.append(nz - i)
    for i in order:
        to_z = (z + i) % nz
        send(
            nrm.at[2 * to_z + c],
            acts.at[c, pl.ds(z * rows, rows), :],
            a_ssem.at[0],
            a_rsem.at[z],
            epid(to_z, x),
            tp,
        )

    def act_block(cc, i):
        return acts.at[cc, pl.ds((z + nz - i) % nz * rows, rows), :]

    def act_pass(i):
        block = act_block(c, i)
        from_z = (z + nz - i) % nz
        arrived(block, a_ssem.at[0], a_rsem.at[from_z])
        send(block, block, ad_ssem.at[0], ad_rsem.at[0], ep, partner)

    w_forward(0)
    w_direct(1)
    phase("acts2")
    for i in order[::-1]:
        act_pass(i)
    phase("weights")
    w_rest(0)
    phase("acts_other")
    arrived(nrm.at[pl.ds(0, nz - 1)], ad_ssem.at[0], ad_rsem.at[0])

    phase("proj0")

    def project(part):
        pbuf[part] = dot(acts[0], wbuf[part, 0:kh, :]) + dot(acts[1], wbuf[part, kh:kz, :])

    chains = ((1, 0, 0), (-1, 0, 1), (-1, 1, 0), (1, 1, 1))
    last = half_z - 1

    def part_rows(part, zz):
        return pbuf[part, pl.ds((zz % nz) * rows, rows), :]

    def ring(n, s):
        d, part, first = chains[n]
        value = part_rows(part, z + nz + d * (half_z - s))
        if s > first:
            arrived(rs_recv.at[n, s - 1], rs_ssem.at[n], rs_rsem.at[n, s - 1])
            value = value + rs_recv[n, s - 1].astype(F32)
        rs_send[n, s] = value.astype(BF16)
        send(
            rs_send.at[n, s],
            rs_recv.at[n, s],
            rs_ssem.at[n],
            rs_rsem.at[n, s],
            epid(z + d + nz, x),
            tp,
        )

    def ring_end(part):
        value = part_rows(part, z)
        for n in (2 * part, 2 * part + 1):
            arrived(rs_recv.at[n, last], rs_ssem.at[n], rs_rsem.at[n, last])
            value = value + rs_recv[n, last].astype(F32)
        return value

    project(0)
    ring(0, 0)
    ring(1, 1)
    phase("w1")
    w_forward(1)
    phase("ring0a")
    ring(0, 1)
    phase("w1rest")
    w_rest(1)
    phase("proj1")
    project(1)
    ring(2, 0)
    ring(3, 1)
    phase("ring2")
    for s in range(2, half_z):
        ring(1, s)
        ring(0, s)
        ring(2, s - 1)
        if s > 2:
            ring(3, s - 1)
    phase("local")
    loads["conv_in"].wait()
    loads["taps"].wait()
    loads["moe_gain"].wait()
    gain2[...] = moe_gain[...].astype(F32)
    tap = taps[...].astype(F32)
    hist = conv_in[0].astype(F32) * tap[0:1]
    for i in (1, 2):
        conv_out[i - 1] = conv_in[i]
        hist = hist + conv_in[i].astype(F32) * tap[i : i + 1]
    loads["routes"].wait()
    loads["prob"].wait()

    phase("ring3")
    proj_x = ring_end(0)
    ring(3, last)
    ring(2, last)

    phase("recur")
    moved = proj_x.astype(BF16)
    conv_out[2] = moved
    conv = (hist + moved.astype(F32) * tap[3:4]).astype(BF16)
    for name in ("rate_w", "input_w", "rate_param", "state_in"):
        loads[name].wait()
    blocks, bw = rate_w.shape[0], rate_w.shape[1]
    rate = jnp.concatenate(
        [dot(conv[:, b * bw : (b + 1) * bw], rate_w[b]) for b in range(blocks)], axis=1
    )
    in_gate = jnp.concatenate(
        [dot(conv[:, b * bw : (b + 1) * bw], input_w[b]) for b in range(blocks)], axis=1
    )
    rate = jax.nn.sigmoid(rate)
    in_gate = jax.nn.sigmoid(in_gate)
    param = rate_param[...]
    soft = jnp.maximum(-param, 0.0) + jnp.log1p(jnp.exp(-jnp.abs(param)))
    log_decay = -8.0 * rate * soft
    tanh_decay = jnp.tanh(log_decay)
    rest = -2.0 * tanh_decay / (1.0 - tanh_decay)
    state = jnp.exp(log_decay) * state_in[...] + jnp.sqrt(rest) * in_gate * conv.astype(F32)
    state_out[...] = state
    phase("ring4")
    proj_y = ring_end(1)
    gelu = 0.5 * proj_y * (
        1.0 + jnp.tanh(0.7978845608028654 * (proj_y + 0.044715 * proj_y * proj_y * proj_y))
    )
    gated = (state * gelu).astype(BF16)

    phase("outproj")
    loads["out_w"].wait()

    def out_cols(yy, cc):
        return pl.ds(pl.multiple_of(tpid(yy, cc) * chan, chan), chan)

    for i in (2, 1, 3, 0):
        os_send[i] = dot(gated, out_w[:, out_cols(y + i, other)]).astype(BF16)
        send(os_send.at[i], os_recv.at[i], os_ssem.at[0], os_rsem.at[i], ep, partner)
    for i in (2, 1, 3):
        value = dot(gated, out_w[:, out_cols(y + i, c)])
        arrived(os_recv.at[i], os_ssem.at[0], os_rsem.at[i])
        oy_send[i] = (value + os_recv[i].astype(F32)).astype(BF16)
        send(oy_send.at[i], oy_recv.at[i], oy_ssem.at[0], oy_rsem.at[i], ep, tpid(y + i, c))
    mixed = tokens[:, out_cols(y, c)].astype(F32) + dot(gated, out_w[:, out_cols(y, c)])

    phase("slots")

    def place(dz):
        return jnp.where(dz <= half_z, jnp.maximum(2 * dz - 1, 0), 2 * (nz - dz))

    offsets = [0]
    for i in range(1, half_z + 1):
        offsets.append(i)
        if i < half_z:
            offsets.append(nz - i)

    experts = lax.broadcasted_iota(jnp.int32, (ep_n, rows), 0)
    chosen = [routes[k : k + 1, :] for k in range(2)]
    one0 = (chosen[0] == experts).astype(F32)
    one1 = (chosen[1] == experts).astype(F32)
    row_ids = lax.broadcasted_iota(jnp.int32, (rows, rows), 0)
    col_ids = lax.broadcasted_iota(jnp.int32, (rows, rows), 1)
    upper = (row_ids < col_ids).astype(F32).astype(BF16)
    before = dot((one0 + one1).astype(BF16), upper)
    ids = lax.broadcasted_iota(jnp.int32, (2 * slots, rows), 0).astype(F32)

    def one_hot(e, one):
        slot = jnp.sum(before * one, axis=0, keepdims=True)
        dz = e // NX - z
        dz = jnp.where(dz < 0, dz + nz, dz)
        block = place(dz) * NX + e % NX
        first = block.astype(F32) * (2.0 * cap) + slot
        return (ids == first).astype(F32), (ids == first + cap).astype(F32)

    lo0, hi0 = one_hot(chosen[0], one0)
    lo1, hi1 = one_hot(chosen[1], one1)
    lo_all = (lo0 + lo1).astype(BF16)
    hi_all = (hi0 + hi1).astype(BF16)

    phase("mixwait")
    arrived(os_recv.at[0], os_ssem.at[0], os_rsem.at[0])
    mixed = mixed + os_recv[0].astype(F32)
    for i in (1, 3, 2):
        arrived(oy_recv.at[i], oy_ssem.at[0], oy_rsem.at[i])
        mixed = mixed + oy_recv[i].astype(F32)
    mixed16 = mixed.astype(BF16)

    phase("dispatch")
    tile = 2 * cap
    per = nz // 2

    def tile_rows(block):
        return pl.ds(pl.multiple_of(block * tile, tile), tile)

    def scatter(g, src, dst, ssem, rsem, sign):
        for j in range(g * per, (g + 1) * per):
            for i in range(NX):
                if j == 0 and i == 0:
                    continue
                to_x = (x + i) % NX
                send(
                    src.at[tile_rows(j * NX + to_x), :],
                    dst.at[tile_rows(j * NX + x), :],
                    ssem.at[0],
                    rsem.at[g],
                    epid(z + nz + sign * offsets[j], to_x),
                    tp,
                )

    def gathered(g, dst, ssem, rsem):
        start = tile if g == 0 else slots
        arrived(dst.at[pl.ds(start, (g + 1) * slots - start), :], ssem.at[0], rsem.at[g])

    def scattered(src, ssem, rsem):
        sent(src.at[pl.ds(tile, 2 * slots - tile), :], ssem.at[0], rsem.at[0])

    for g in range(2):
        part = slice(g * slots, (g + 1) * slots)
        sd[part, :] = (
            dot(lo_all[part], mixed16[:, 0:ch]) + dot(hi_all[part], mixed16[:, ch:chan])
        ).astype(BF16)
        scatter(g, sd, gbuf.at[tp], s_ssem, s_rsem, 1)
    gbuf[tp, tile_rows(x), :] = sd[tile_rows(x), :]

    hs = slots // 2

    def piece_of(t, g, q):
        return gbuf.at[t, pl.ds(g * slots + q * hs, hs), :]

    def share(t, g, q, to_tp):
        ref = piece_of(t, g, q)
        rsem = ao_rsem.at[t // NC, g] if to_tp is partner else ag_rsem.at[t // NC, g, q]
        send(ref, ref, ag_ssem.at[g], rsem, ep, to_tp)

    def shared(t, g, q):
        arrived(piece_of(t, g, q), ag_ssem.at[g], ag_rsem.at[t // NC, g, q])

    def shared_other(t, g):
        both = gbuf.at[t, pl.ds(g * slots, slots), :]
        arrived(both, ag_ssem.at[g], ao_rsem.at[t // NC, g])

    up_tp = tpid(y + 1, c)
    down_tp = tpid(y + 3, c)
    far_tp = tpid(y + 2, c)

    def own_share(g):
        share(tp, g, 0, up_tp)
        share(tp, g, 1, down_tp)
        share(tp, g, 1, up_tp)
        share(tp, g, 0, down_tp)
        share(tp, g, 0, partner)
        share(tp, g, 1, partner)

    def near_share(g):
        shared(down_tp, g, 0)
        share(down_tp, g, 0, up_tp)
        share(down_tp, g, 0, partner)
        shared(up_tp, g, 1)
        share(up_tp, g, 1, down_tp)
        share(up_tp, g, 1, partner)
        shared(down_tp, g, 1)
        share(down_tp, g, 1, partner)
        shared(up_tp, g, 0)
        share(up_tp, g, 0, partner)

    def far_share(g):
        for q in range(2):
            shared(far_tp, g, q)
            share(far_tp, g, q, partner)

    squares = [jnp.zeros((hs, 1), F32), jnp.zeros((hs, 1), F32)]

    def absorb(t, g, first=False):
        value = gbuf[t, g * slots : (g + 1) * slots, :].astype(F32)
        value = value.reshape(ep_n // 2, tile, ch)
        parts = (value[:, 0:cap, :], value[:, cap:, :])
        for k in range(2):
            piece = parts[k].reshape(hs, ch)
            squares[g] = squares[g] + jnp.sum(piece * piece, axis=1, keepdims=True)
            lanes = []
            for j in range(ch // 128):
                row = gain2[pl.ds(t * (chan // 128) + (k * ch) // 128 + j, 1), :]
                lanes.append((piece[:, j * 128 : (j + 1) * 128] * row).astype(BF16))
            at = pl.multiple_of(t * chan + k * ch, ch)
            product = dot(jnp.concatenate(lanes, axis=1), wgu[pl.ds(at, ch), :])
            if first and k == 0:
                acc[g] = product
            else:
                acc[g] += product

    def absorb_other(i, g):
        t = tpid(y + i, other)
        shared_other(t, g)
        absorb(t, g)

    def hidden_of(g):
        scale2 = lax.rsqrt(squares[g] * (1.0 / width) + 1e-06)
        gate_part = acc[g, :, 0:ff] * scale2
        up_part = acc[g, :, ff:] * scale2
        return (gate_part * jax.nn.sigmoid(gate_part) * up_part).astype(BF16)

    hq = hs // 2

    def down_send(g, hidden):
        for i in (2, 1, 3, 0):
            d_send[g, i] = dot(hidden, wd[:, out_cols(y + i, other)]).astype(BF16)
            send(d_send.at[g, i], d_recv.at[g, i], d_ssem.at[g], d_rsem.at[g, i], ep, partner)

    def own_part(g, hidden, i):
        value = dot(hidden, wd[:, out_cols(y + i, c)])
        arrived(d_recv.at[g, i], d_ssem.at[g], d_rsem.at[g, i])
        return value + d_recv[g, i].astype(F32)

    def q_out(g, n, value, dst, rsem, to_tp):
        q_send[g, n] = value.astype(BF16)
        send(q_send.at[g, n], dst, q_ssem.at[g], rsem, ep, to_tp)

    def rs_first(g, hidden):
        value = own_part(g, hidden, 2)
        q_out(g, 0, value[0:hq], fw_recv.at[g, 0], fw_rsem.at[g, 0], up_tp)
        q_out(g, 1, value[hq:], fw_recv.at[g, 1], fw_rsem.at[g, 1], down_tp)
        value = own_part(g, hidden, 1)
        q_out(g, 2, value[hq:], fin_recv.at[g, 1, 0], fin_rsem.at[g, 1], up_tp)
        qf[g, 0] = value[0:hq]
        value = own_part(g, hidden, 3)
        q_out(g, 3, value[0:hq], fin_recv.at[g, 0, 1], fin_rsem.at[g, 0], down_tp)
        qf[g, 1] = value[hq:]
        qf[g, 2] = own_part(g, hidden, 0)[0:hq]
        qf[g, 3] = own_rest(g, hidden)

    def own_rest(g, hidden):
        return dot(hidden[hq:], wd[:, out_cols(y, c)]) + d_recv[g, 0, hq:, :].astype(F32)

    def rs_forward(g):
        arrived(fw_recv.at[g, 0], q_ssem.at[g], fw_rsem.at[g, 0])
        value = qf[g, 0] + fw_recv[g, 0].astype(F32)
        q_out(g, 4, value, fin_recv.at[g, 0, 0], fin_rsem.at[g, 0], up_tp)
        arrived(fw_recv.at[g, 1], q_ssem.at[g], fw_rsem.at[g, 1])
        value = qf[g, 1] + fw_recv[g, 1].astype(F32)
        q_out(g, 5, value, fin_recv.at[g, 1, 1], fin_rsem.at[g, 1], down_tp)

    def rs_final(g):
        for h in range(2):
            arrived(fin_recv.at[g, h], q_ssem.at[g], fin_rsem.at[g, h])
            total = qf[g, 2 + h] + fin_recv[g, h, 0].astype(F32) + fin_recv[g, h, 1].astype(F32)
            total = total.reshape(hq // cap, cap, chan)
            total = jnp.concatenate([total[:, :, 0:ch], total[:, :, ch:]], axis=1)
            at = g * slots + h * hs
            back_send[at : at + hs, :] = total.reshape(hs, ch).astype(BF16)

    phase("a2a_wait0")
    gathered(0, gbuf.at[tp], s_ssem, s_rsem)
    own_share(0)
    phase("absorb0")
    loads["eg"].wait()
    loads["eu"].wait()
    loads["ed"].wait()
    absorb(tp, 0, True)
    absorb_other(0, 0)
    phase("near0")
    near_share(0)
    phase("a2a_wait1")
    gathered(1, gbuf.at[tp], s_ssem, s_rsem)
    own_share(1)
    phase("absorb_near0")
    absorb(down_tp, 0)
    absorb(up_tp, 0)
    phase("far0")
    far_share(0)
    phase("other0")
    absorb_other(3, 0)
    absorb_other(1, 0)
    absorb(far_tp, 0)
    absorb_other(2, 0)
    phase("hidden0")
    hidden0 = hidden_of(0)
    down_send(0, hidden0)
    phase("near1")
    near_share(1)
    phase("rs_first0")
    rs_first(0, hidden0)
    phase("absorb1")
    absorb(tp, 1, True)
    absorb_other(0, 1)
    absorb(down_tp, 1)
    absorb(up_tp, 1)
    phase("far1")
    far_share(1)
    phase("other1")
    absorb_other(3, 1)
    absorb_other(1, 1)
    absorb(far_tp, 1)
    absorb_other(2, 1)
    phase("hidden1")
    hidden1 = hidden_of(1)
    down_send(1, hidden1)
    phase("rs_fw0")
    rs_forward(0)
    phase("rs_first1")
    rs_first(1, hidden1)
    phase("rs_fin0")
    rs_final(0)
    scatter(0, back_send, back_recv, b_ssem, b_rsem, -1)
    phase("rs_fw1")
    rs_forward(1)
    back_recv[tile_rows(x), :] = back_send[tile_rows(x), :]
    total = prob[0:1, :] + prob[1:2, :]
    eye = row_ids == col_ids

    def column(row):
        return jnp.sum(jnp.where(eye, row, 0.0), axis=1, keepdims=True)

    w0 = column(prob[0:1, :] / total)
    w1 = column(prob[1:2, :] / total)
    phase("rs_fin1")
    rs_final(1)
    scatter(1, back_send, back_recv, b_ssem, b_rsem, -1)
    phase("back_wait0")
    gathered(0, back_recv, b_ssem, b_rsem)
    phase("back_wait1")
    gathered(1, back_recv, b_ssem, b_rsem)
    phase("combine")
    returned = back_recv[...]
    for k, (a, b) in enumerate(((lo0, lo1), (hi0, hi1))):
        picked = w0 * dot_t(a.astype(BF16), returned) + w1 * dot_t(b.astype(BF16), returned)
        layer_out[:, k * ch : (k + 1) * ch] = (
            mixed[:, k * ch : (k + 1) * ch] + picked
        ).astype(BF16)

    phase("drain")
    for part in range(2):
        sent(wbuf.at[part, pl.ds(0, 6 * hk), :], w_ssem.at[part], w_rsem.at[part, 0, 0])
    sent(nrm.at[pl.ds(0, nz - 1)], a_ssem.at[0], a_rsem.at[0])
    sent(nrm.at[pl.ds(0, nz - 1)], ad_ssem.at[0], ad_rsem.at[0])
    for n in range(4):
        first = chains[n][2]
        sent(rs_send.at[n, pl.ds(first, half_z - first)], rs_ssem.at[n], rs_rsem.at[n, 0])
    sent(os_send, os_ssem.at[0], os_rsem.at[0])
    sent(oy_send.at[pl.ds(1, NY - 1)], oy_ssem.at[0], oy_rsem.at[0])
    scattered(sd, s_ssem, s_rsem)
    for g in range(2):
        sent(gbuf.at[pl.ds(0, 7), pl.ds(0, slots), :], ag_ssem.at[g], ag_rsem.at[0, g, 0])
        sent(d_send.at[g], d_ssem.at[g], d_rsem.at[g, 0])
        sent(q_send.at[g], q_ssem.at[g], fw_rsem.at[g, 0])
    scattered(back_send, b_ssem, b_rsem)
    phase(None)


def finish_kernel(a, b, c, a_out, b_out, c_out, sems):
    copies = [
        pltpu.make_async_copy(src, dst, sems.at[n])
        for n, (src, dst) in enumerate(((a, a_out), (b, b_out), (c, c_out)))
    ]
    for copy in copies:
        copy.start()
    for copy in copies:
        copy.wait()


def shards(
    tokens,
    state_in,
    conv_in,
    mix_gain,
    rnn_weight,
    gate_weight,
    conv_weight,
    rate_weight,
    input_weight,
    rate_param,
    out_weight,
    moe_gain,
    expert_gate,
    expert_up,
    expert_down,
    routes,
    route_prob,
):
    rows, width = tokens.shape
    ks, chan = rnn_weight.shape
    ep_n = lax.axis_size("ep")
    tp_n = lax.axis_size("tp")
    nz = ep_n // NX
    half_z = nz // 2
    kh = width // nz // 2
    ff = expert_down.shape[1]
    topk = routes.shape[1]
    cap = max(2, 2 * rows * topk // ep_n)
    slots = ep_n * cap
    hs = slots // 2
    ch = chan // 2

    vm = pl.BlockSpec(memory_space=pltpu.VMEM)
    hbm = pl.BlockSpec(memory_space=pltpu.HBM)
    dma = pltpu.SemaphoreType.DMA
    shapes = (
        jax.ShapeDtypeStruct((rows, chan), BF16),
        jax.ShapeDtypeStruct((rows, chan), F32),
        jax.ShapeDtypeStruct((3, rows, chan), BF16),
    )
    outs = pl.pallas_call(
        layer_kernel,
        out_shape=tuple(pltpu.VMEM(a.shape, a.dtype) for a in shapes),
        in_specs=[hbm] * 17,
        out_specs=(vm, vm, vm),
        scratch_shapes=[
            pltpu.VMEM((rows, width), BF16),
            pltpu.VMEM((3, rows, chan), BF16),
            pltpu.VMEM((rows, chan), F32),
            pltpu.VMEM((width // 128, 128), BF16),
            pltpu.VMEM((4, chan), BF16),
            pltpu.VMEM(rate_weight.shape, BF16),
            pltpu.VMEM(input_weight.shape, BF16),
            pltpu.VMEM((1, chan), F32),
            pltpu.VMEM((width // 128, 128), BF16),
            pltpu.VMEM((topk, rows), jnp.int32),
            pltpu.VMEM((topk, rows), F32),
            pltpu.VMEM((chan, width), BF16),
            pltpu.VMEM((width, 2 * ff), BF16),
            pltpu.VMEM((ff, width), BF16),
            pltpu.VMEM((2 * nz, rows, kh), BF16),
            pltpu.VMEM((2, nz * rows, kh), BF16),
            pltpu.VMEM((2, NX * ks, chan), BF16),
            pltpu.VMEM((2, nz * rows, chan), F32),
            pltpu.VMEM((4, half_z, rows, chan), BF16),
            pltpu.VMEM((4, half_z, rows, chan), BF16),
            pltpu.VMEM((NY, rows, chan), BF16),
            pltpu.VMEM((NY, rows, chan), BF16),
            pltpu.VMEM((NY, rows, chan), BF16),
            pltpu.VMEM((NY, rows, chan), BF16),
            pltpu.VMEM((2 * slots, ch), BF16),
            pltpu.VMEM((tp_n, 2 * slots, ch), BF16),
            pltpu.VMEM((width // 128, 128), F32),
            pltpu.VMEM((2, hs, 2 * ff), F32),
            pltpu.VMEM((2, NY, hs, chan), BF16),
            pltpu.VMEM((2, NY, hs, chan), BF16),
            pltpu.VMEM((2, 4, hs // 2, chan), F32),
            pltpu.VMEM((2, 6, hs // 2, chan), BF16),
            pltpu.VMEM((2, 2, hs // 2, chan), BF16),
            pltpu.VMEM((2, 2, 2, hs // 2, chan), BF16),
            pltpu.VMEM((2 * slots, ch), BF16),
            pltpu.VMEM((2 * slots, ch), BF16),
            dma((17,)),
            dma((2,)),
            dma((2, NX, 2)),
            dma((1,)),
            dma((nz,)),
            dma((1,)),
            dma((1,)),
            dma((4,)),
            dma((4, half_z)),
            dma((1,)),
            dma((NY,)),
            dma((1,)),
            dma((NY,)),
            dma((1,)),
            dma((2,)),
            dma((2,)),
            dma((NY, 2, 2)),
            dma((NY, 2)),
            dma((2,)),
            dma((2, NY)),
            dma((2,)),
            dma((2, 2)),
            dma((2, 2)),
            dma((1,)),
            dma((2,)),
        ],
        compiler_params=pltpu.CompilerParams(
            collective_id=0,
            has_side_effects=True,
            vmem_limit_bytes=66000000,
        ),
        name="layer",
    )(
        tokens,
        conv_in.transpose(1, 0, 2),
        state_in,
        mix_gain.reshape(width // 128, 128),
        rnn_weight,
        gate_weight,
        conv_weight,
        rate_weight,
        input_weight,
        rate_param.reshape(1, chan),
        moe_gain.reshape(width // 128, 128),
        routes.T,
        route_prob.T,
        out_weight,
        expert_gate,
        expert_up,
        expert_down,
    )
    layer_out, state_out, conv_out = pl.pallas_call(
        finish_kernel,
        out_shape=shapes,
        in_specs=[vm] * 3,
        out_specs=(hbm, hbm, hbm),
        scratch_shapes=[dma((3,))],
        compiler_params=pltpu.CompilerParams(vmem_limit_bytes=4 * 1024 * 1024),
        name="finish",
    )(*outs)
    return (layer_out, state_out, conv_out.transpose(1, 0, 2))


def solution(mesh):
    in_specs = (
        P("ep", None),
        P("ep", "tp"),
        P("ep", None, "tp"),
        P(),
        P("ep", "tp"),
        P("ep", "tp"),
        P(None, "tp"),
        P("tp", None, None),
        P("tp", None, None),
        P("tp"),
        P("tp", None),
        P(),
        P("ep", None, "tp"),
        P("ep", None, "tp"),
        P("ep", "tp", None),
        P("ep", None),
        P("ep", None),
    )
    out_specs = (P("ep", "tp"), P("ep", "tp"), P("ep", None, "tp"))
    return jax.shard_map(shards, mesh=mesh, in_specs=in_specs, out_specs=out_specs, check_vma=False)
```

time: 101 us -> 91.1 us (0.902)
  the two profiles are of different devices: /device:TPU:1 before, /device:TPU:8 now
where the time goes in v3:
time: 91.1 us
  Pallas kernels  90.4 us (99%)
    pallas_call x1, Pallas kernels, shards(): pl.pallas_call(layer_kernel, out_shape=tuple((pltpu.VMEM(a.shape, a.dtype...  89.6 us

profile of v3, /device:TPU:8, one launch (start us, length us, event | category | flops | bytes accessed | tf_op | source)
XLA Modules:
  0.0 91.1 jit_solution(17888920645959863506)
XLA Ops:
  0.6 89.6 %layer.1 = (bf16[64,512]{1,0:T(8,128)(2,1)S(1)}, f32[64,512]{1,0:T(8,128)S(1)}, bf16[3,64,512]{2,1,0:T(8,128)(2,1)S(1)}) custom-call(bf16[64,4096]{1,0:T(8,128)(2,1)} %tokens_hbm.1, bf16[3,64,512]{2,1,0:T(8,128)(2,1)} %bitcast.7, f32[64,512]{1,0:T(8,128)} %state_in_hbm.1, bf16[32,128]{1,0:T(8,128)(2,1)} %bitcast.8, bf16[128,512]{1,0:T(8,128)(2,1)} %rnn_w_hbm.1, ...), custom_call_target="tpu_custom_call" | custom-call | tf_op jit(solution)/shard_map/layer/pallas_call | solution.py:786
  90.3 0.8 finish.1
